TPU v7x, 32 devices: a whole 2x2x4 slice. The times are simulated.
32 devices in a mesh: grp: 2 (over y), fs: 4 (over z), tp: 4 (over x, core).
Axes of the slice: x: 2, y: 2, z: 4, core: 2. Of those that a mesh axis runs over, the one named last changes fastest.
Arguments:
- tokens: bfloat16 [8192, 2048], P(('grp', 'fs'), 'tp'), parts along dimension 0, may hold values from -6 to 6
- norm1_gain: float32 [2048], replicated, may hold values from 0.1 to 1.9
- weight_u: float32 [2048, 1024], P('fs', 'tp'), may hold values from -0.125 to 0.125
- weight_v: float32 [2048, 1024], P('fs', 'tp'), may hold values from -0.125 to 0.125
- scale_u: float32 [1024], P('tp'), may hold values from 0.5 to 2
- scale_v: float32 [1024], P('tp'), may hold values from 0.05 to 4.5
- mix_gain: float32 [1024], P('tp'), may hold values from 0.1 to 1.9
- spatial_weight: float32 [4, 128, 128], replicated, may hold values from -0.5 to 0.5
- spatial_bias: float32 [4, 128], replicated, may hold values from 0.5 to 1.5
- weight_out: float32 [1024, 2048], P('tp', 'fs'), may hold values from -0.1875 to 0.1875
- scale_out: float32 [2048], P('fs'), may hold values from 0.5 to 2
- norm2_gain: float32 [2048], replicated, may hold values from 0.1 to 1.9
- weight_up: float32 [2048, 8192], P('fs', 'tp'), may hold values from -0.125 to 0.125
- scale_up: float32 [8192], P('tp'), may hold values from 0.5 to 2
- weight_down: float32 [8192, 2048], P('tp', 'fs'), may hold values from -0.0625 to 0.0625
- scale_down: float32 [2048], P('fs'), may hold values from 0.5 to 2
Outputs:
- result: bfloat16 [8192, 2048], P(('grp', 'fs'), 'tp'), parts along dimension 0
There are 2 independent parts, one for each index of `grp`. A program takes and returns all parts, laid end to end along the dimension named above; an argument that names none is the same for every part. Nothing has to cross between parts.
All inputs are finite; a program needn't handle non-finite values.
Results may differ from a plain program's by a relative error of at most 0.023.
Values may be sent and summed in bfloat16 or wider, within the bound.
A program may use at most 128 MiB of HBM per device.

v0:
```python
import jax
import jax.numpy as jnp
from jax import lax
from jax.sharding import PartitionSpec as P

GM_W = 1024
GROUPS = 4
BLOCK = 128


def per_device(
    tokens,
    norm1_gain,
    weight_u,
    weight_v,
    scale_u,
    scale_v,
    mix_gain,
    spatial_weight,
    spatial_bias,
    weight_out,
    scale_out,
    norm2_gain,
    weight_up,
    scale_up,
    weight_down,
    scale_down,
):
    feature_count = norm1_gain.shape[0]
    out_scales, down_scales = (
        lax.all_gather(scale_out, "fs", axis=0, tiled=True),
        lax.all_gather(scale_down, "fs", axis=0, tiled=True),
    )
    full_u, full_v = (
        lax.all_gather(weight_u.astype(jnp.bfloat16), "fs", axis=0, tiled=True),
        lax.all_gather(weight_v.astype(jnp.bfloat16), "fs", axis=0, tiled=True),
    )
    widened_in = tokens.astype(jnp.float32)
    squares_in = lax.psum(jnp.sum(widened_in * widened_in, axis=1), "tp")
    inverse_in = lax.rsqrt(squares_in / feature_count + 1e-06)[:, None]
    gain_piece = norm1_gain
    normed_piece = (
        lax.all_gather(tokens, "tp", axis=1, tiled=True).astype(jnp.float32)
        * inverse_in
        * gain_piece
    ).astype(jnp.bfloat16)
    pre_u = jnp.dot(normed_piece, full_u, preferred_element_type=jnp.float32)
    pre_v = jnp.dot(normed_piece, full_v, preferred_element_type=jnp.float32)
    gate_u = jax.nn.gelu(pre_u * scale_u)
    act_v = jax.nn.gelu(pre_v * scale_v)
    local_width = act_v.shape[1]
    row_sums, row_squares = lax.psum((jnp.sum(act_v, axis=1), jnp.sum(act_v * act_v, axis=1)), "tp")
    row_mean = (row_sums / GM_W)[:, None]
    square = (row_squares / GM_W)[:, None]
    v_norm = (
        (act_v - row_mean) * lax.rsqrt(square - row_mean * row_mean + 1e-06) * mix_gain
    ).astype(jnp.bfloat16)
    group_index = lax.axis_index("tp") * local_width // (GM_W // GROUPS)
    lower_mask = jnp.tril(jnp.ones((BLOCK, BLOCK), jnp.float32))
    spatial_mask = (
        lax.dynamic_index_in_dim(spatial_weight, group_index, 0, keepdims=False) * lower_mask
    ).astype(jnp.bfloat16)
    block_bias = lax.dynamic_index_in_dim(spatial_bias, group_index, 0, keepdims=False)
    blocks = v_norm.reshape(-1, BLOCK, local_width)
    mixed_cols = jnp.einsum("ts,nsc->ntc", spatial_mask, blocks, preferred_element_type=jnp.float32)
    mixed_cols = mixed_cols + block_bias[None, :, None]
    gated = (gate_u * mixed_cols.reshape(-1, local_width)).astype(jnp.bfloat16)
    out_rounded = weight_out.astype(jnp.bfloat16)
    full_out = lax.all_gather(out_rounded, "fs", axis=1, tiled=True)
    columns = full_out
    piece_scale = out_scales
    product = lax.dot_general(
        columns, gated, (((0,), (1,)), ((), ())), preferred_element_type=jnp.float32
    )
    mixer_sum = (
        lax.psum_scatter(
            (product * piece_scale[:, None]).astype(jnp.bfloat16),
            "tp",
            scatter_dimension=0,
            tiled=True,
        )
        .astype(jnp.float32)
        .T
    )
    residual = (tokens.astype(jnp.float32) + mixer_sum).astype(jnp.bfloat16)
    full_up = lax.all_gather(weight_up.astype(jnp.bfloat16), "fs", axis=0, tiled=True)
    widened_mid = residual.astype(jnp.float32)
    squares_mid = lax.psum(jnp.sum(widened_mid * widened_mid, axis=1), "tp")
    inverse_mid = lax.rsqrt(squares_mid / feature_count + 1e-06)[:, None]
    gain_piece = norm2_gain
    normed_piece = (
        lax.all_gather(residual, "tp", axis=1, tiled=True).astype(jnp.float32)
        * inverse_mid
        * gain_piece
    ).astype(jnp.bfloat16)
    pre_up = jnp.dot(normed_piece, full_up, preferred_element_type=jnp.float32)
    hidden = jnp.square(jax.nn.relu(pre_up * scale_up)).astype(jnp.bfloat16)
    down_rounded = weight_down.astype(jnp.bfloat16)
    full_down = lax.all_gather(down_rounded, "fs", axis=1, tiled=True)
    columns = full_down
    piece_scale = down_scales
    product = lax.dot_general(
        columns, hidden, (((0,), (1,)), ((), ())), preferred_element_type=jnp.float32
    )
    channel_sum = (
        lax.psum_scatter(
            (product * piece_scale[:, None]).astype(jnp.bfloat16),
            "tp",
            scatter_dimension=0,
            tiled=True,
        )
        .astype(jnp.float32)
        .T
    )
    return (residual.astype(jnp.float32) + channel_sum).astype(jnp.bfloat16)


def solution(mesh):
    placed = (
        P(("grp", "fs"), "tp"),
        P(),
        P("fs", "tp"),
        P("fs", "tp"),
        P("tp"),
        P("tp"),
        P("tp"),
        P(),
        P(),
        P("tp", "fs"),
        P("fs"),
        P(),
        P("fs", "tp"),
        P("tp"),
        P("tp", "fs"),
        P("fs"),
    )
    return jax.shard_map(
        per_device, mesh=mesh, in_specs=placed, out_specs=P(("grp", "fs"), "tp"), check_vma=False
    )
```

profile of v0, /device:TPU:0, one launch (start us, length us, event | category | flops | bytes accessed | tf_op | source)
XLA Modules:
  0.0 601.0 jit_solution(15916655100287442903)
XLA Ops:
  6.5 1.8 convert_element_type.74
  8.3 0.0 all-gather.14.cloned.1.call-update
  8.3 0.0 all-gather.10.cloned.1.call-start
  8.4 0.7 all-gather.10.cloned.1.call-update
  9.1 0.0 all-gather.12.cloned.1.call-start
  9.1 1.8 convert_element_type.73
  10.9 0.0 all-gather.12.cloned.1.call-update
  10.9 0.0 all-gather.16.cloned.1.call-start
  11.0 1.8 convert_element_type.79
  12.7 0.0 all-gather.16.cloned.1.call-update
  12.8 0.0 reduce-scatter.3.cloned.1.call-start
  12.8 1.5 fusion.8
  14.3 8.4 %psum.28 = f32[1024]{0:T(1024)S(1)} all-reduce(f32[1024]{0:T(1024)S(1)} %fusion.8), channel_id=1, replica_groups=mesh['grp'=2,'fs'=4,'tp'=4] {'tp'}, use_global_device_ids=true, to_apply=%region_1.0 | all-reduce | flops 1024 | bytes 8192 | tf_op jit(solution)/shard_map/psum | solution.py:39
  22.7 12.7 %all-gather = f32[4,1,512]{2,1,0:T(1,128)S(1)} all-gather(f32[1,1,512]{2,1,0:T(1,128)} %bitcast.33), channel_id=1, replica_groups=mesh['grp'=2,'fs'=4,'tp'=4] {'fs'}, dimensions={0}, use_global_device_ids=true | all-gather | bytes 10240 | tf_op jit(solution)/shard_map/all_gather | solution.py:31
  35.4 0.0 copy-start.4
  35.4 0.0 copy-start.5
  35.4 0.0 copy-start.8
  35.5 4.3 all-gather.14.cloned.1.call-done
  39.8 35.4 %all-gather.10.cloned.1.call-done = bf16[1024,2048]{1,0:T(8,128)(2,1)} async-done(((bf16[1024,512]{1,0:T(8,128)(2,1)}), bf16[1024,2048]{1,0:T(8,128)(2,1)}) %all-gather.10.cloned.1.call-update) | async-done | bytes 4194320 | tf_op jit(solution)/shard_map/all_gather | solution.py:43
  75.2 4.2 fusion.45
  79.4 6.0 %all-reduce = (f32[1024]{0:T(1024)S(1)}, f32[1024]{0:T(1024)S(1)}) all-reduce(f32[1024]{0:T(1024)S(1)} %get-tuple-element.6, f32[1024]{0:T(1024)S(1)} %get-tuple-element.5), channel_id=1, replica_groups=mesh['grp'=2,'fs'=4,'tp'=4] {'tp'}, use_global_device_ids=true, to_apply=%region_5.0 | all-reduce | flops 2048 | bytes 16384 | tf_op jit(solution)/shard_map/psum | solution.py:52
  85.4 0.3 multiply_convert_fusion.21
  85.8 1.1 convolution_add_fusion
  86.9 17.9 %all-gather.12.cloned.1.call-done = bf16[2048,256]{1,0:T(8,128)(2,1)} async-done(((bf16[512,256]{1,0:T(8,128)(2,1)}), bf16[2048,256]{1,0:T(8,128)(2,1)}) %all-gather.12.cloned.1.call-update) | async-done | bytes 1048592 | tf_op jit(solution)/shard_map/all_gather | solution.py:35
  104.8 28.8 %all-gather.16.cloned.1.call-done = bf16[256,2048]{1,0:T(8,128)(2,1)} async-done(((bf16[256,512]{1,0:T(8,128)(2,1)}), bf16[256,2048]{1,0:T(8,128)(2,1)}) %all-gather.16.cloned.1.call-update) | async-done | bytes 1048592 | tf_op jit(solution)/shard_map/all_gather | solution.py:69
  133.6 9.3 %fusion.6 = bf16[2048,1024]{0,1:T(8,128)(2,1)} fusion(f32[2048]{0:T(1024)S(1)} %bitcast.31, bf16[256,2048]{1,0:T(8,128)(2,1)} %all-gather.16.cloned.1.call-done, f32[1024,256]{1,0:T(8,128)S(1)} %bitcast.30, bf16[2048,256]{1,0:T(8,128)(2,1)} %all-gather.12.cloned.1.call-done, bf16[1024,2048]{1,0:T(8,128)(2,1)} %all-gather.10.cloned.1.call-done, ...), kind=kOutput, calls=%fused_computation.9 | convolution fusion | flops 2162950144 | bytes 11555840 | tf_op jit(solution)/shard_map/dot_general | solution.py:72
  142.9 0.0 reduce-scatter.3.cloned.1.call-update
  142.9 0.0 copy-start.2
  142.9 0.0 all-gather.20.cloned.1.call-start
  143.0 3.9 convert_element_type.86
  146.9 0.0 all-gather.20.cloned.1.call-update
  146.9 0.0 all-gather.22.cloned.1.call-start
  147.0 4.4 convert_element_type.88
  151.4 0.0 all-gather.22.cloned.1.call-update
  151.4 0.0 all-gather.18.cloned.1.call-start
  151.5 35.4 %reduce-scatter.3.cloned.1.call-done = bf16[512,1024]{0,1:T(8,128)(2,1)} async-done(((bf16[2048,1024]{0,1:T(8,128)(2,1)}), bf16[512,1024]{0,1:T(8,128)(2,1)}) %reduce-scatter.3.cloned.1.call-update) | async-done | bytes 1048592 | tf_op jit(solution)/shard_map/reduce_scatter | solution.py:76
  186.8 2.6 fusion.10
  189.4 0.0 all-gather.18.cloned.1.call-update
  189.5 0.0 reduce-scatter.5.cloned.1.call-start
  189.5 12.0 %all-gather.1 = f32[4,1,512]{2,1,0:T(1,128)S(1)} all-gather(f32[1,1,512]{2,1,0:T(1,128)S(1)} %bitcast.34), channel_id=1, replica_groups=mesh['grp'=2,'fs'=4,'tp'=4] {'fs'}, dimensions={0}, use_global_device_ids=true | all-gather | bytes 10240 | tf_op jit(solution)/shard_map/all_gather | solution.py:32
  201.5 6.0 %psum.31 = f32[1024]{0:T(1024)S(1)} all-reduce(f32[1024]{0:T(1024)S(1)} %get-tuple-element.9), channel_id=1, replica_groups=mesh['grp'=2,'fs'=4,'tp'=4] {'tp'}, use_global_device_ids=true, to_apply=%region_8.9 | all-reduce | flops 1024 | bytes 8192 | tf_op jit(solution)/shard_map/psum | solution.py:88
  207.6 130.4 %all-gather.20.cloned.1.call-done = bf16[2048,2048]{1,0:T(8,128)(2,1)} async-done(((bf16[512,2048]{1,0:T(8,128)(2,1)}), bf16[2048,2048]{1,0:T(8,128)(2,1)}) %all-gather.20.cloned.1.call-update) | async-done | bytes 8388624 | tf_op jit(solution)/shard_map/all_gather | solution.py:86
  337.9 149.4 %all-gather.22.cloned.1.call-done = bf16[2048,2048]{1,0:T(8,128)(2,1)} async-done(((bf16[2048,512]{1,0:T(8,128)(2,1)}), bf16[2048,2048]{1,0:T(8,128)(2,1)}) %all-gather.22.cloned.1.call-update) | async-done | bytes 8388624 | tf_op jit(solution)/shard_map/all_gather | solution.py:99
  487.3 34.2 %all-gather.18.cloned.1.call-done = bf16[1024,2048]{1,0:T(8,128)(2,1)} async-done(((bf16[1024,512]{1,0:T(8,128)(2,1)}), bf16[1024,2048]{1,0:T(8,128)(2,1)}) %all-gather.18.cloned.1.call-update) | async-done | bytes 4194320 | tf_op jit(solution)/shard_map/all_gather | solution.py:92
  521.6 25.7 %fusion.7 = bf16[2048,1024]{0,1:T(8,128)(2,1)} fusion(f32[2048]{0:T(1024)S(1)} %bitcast.32, bf16[2048,2048]{1,0:T(8,128)(2,1)} %all-gather.22.cloned.1.call-done, bf16[2048,2048]{1,0:T(8,128)(2,1)} %all-gather.20.cloned.1.call-done, bf16[1024,2048]{1,0:T(8,128)(2,1)} %all-gather.18.cloned.1.call-done, f32[2048]{0:T(1024)S(1)} %copy-done.6, ...), kind=kOutput, calls=%fused_computation.10 | convolution fusion | flops 17200840704 | bytes 25194496 | tf_op jit(solution)/shard_map/dot_general | solution.py:102
  547.3 0.0 reduce-scatter.5.cloned.1.call-update
  547.3 44.6 %reduce-scatter.5.cloned.1.call-done = bf16[512,1024]{0,1:T(8,128)(2,1)} async-done(((bf16[2048,1024]{0,1:T(8,128)(2,1)}), bf16[512,1024]{0,1:T(8,128)(2,1)}) %reduce-scatter.5.cloned.1.call-update) | async-done | bytes 1048592 | tf_op jit(solution)/shard_map/reduce_scatter | solution.py:106
  591.9 2.5 fusion.11
  (19 shorter events, 0.1 us)
Async XLA Ops:
  6.5 28.9 %copy-start = (f32[4,128]{1,0:T(4,128)S(1)}, f32[4,128]{1,0:T(4,128)}, u32[]{:S(2)}) copy-start(f32[4,128]{1,0:T(4,128)} %param.24) | copy-start | bytes 6148
  6.5 33.2 %all-gather.14.cloned.1.call-start = ((), (), s32[]{:S(2)}) async-start(), calls=%async_computation.4 | async-start | bytes 1310720 | tf_op jit(solution)/shard_map/all_gather | solution.py:36
  8.3 66.9 %all-gather.10.cloned.1.call-start = ((), (), s32[]{:S(2)}) async-start(), calls=%async_computation.2 | async-start | bytes 5242880 | tf_op jit(solution)/shard_map/all_gather | solution.py:43
  9.1 95.7 %all-gather.12.cloned.1.call-start = ((), (), s32[]{:S(2)}) async-start(), calls=%async_computation.3 | async-start | bytes 1310720 | tf_op jit(solution)/shard_map/all_gather | solution.py:35
  10.9 122.7 %all-gather.16.cloned.1.call-start = ((), (), s32[]{:S(2)}) async-start(), calls=%async_computation.5 | async-start | bytes 1310720 | tf_op jit(solution)/shard_map/all_gather | solution.py:69
  12.8 174.1 %reduce-scatter.3.cloned.1.call-start = ((), (), s32[]{:S(2)}) async-start(), calls=%async_computation.6 | async-start | bytes 5242880 | tf_op jit(solution)/shard_map/reduce_scatter | solution.py:76
  35.4 50.0 %copy-start.4 = (f32[256]{0:T(256)S(1)}, f32[256]{0:T(256)}, u32[]{:S(2)}) copy-start(f32[256]{0:T(256)} %param.22) | copy-start | bytes 3076
  35.4 98.2 %copy-start.5 = (f32[2048]{0:T(1024)S(1)}, f32[2048]{0:T(1024)}, u32[]{:S(2)}) copy-start(f32[2048]{0:T(1024)} %param.17) | copy-start | bytes 24580
  35.4 98.2 %copy-start.8 = (f32[256]{0:T(256)S(1)}, f32[256]{0:T(256)}, u32[]{:S(2)}) copy-start(f32[256]{0:T(256)} %param.20) | copy-start | bytes 3076
  142.9 43.9 %copy-start.2 = (bf16[1024,512]{1,0:T(8,128)(2,1)S(1)}, bf16[1024,512]{1,0:T(8,128)(2,1)}, u32[]{:S(2)}) copy-start(bf16[1024,512]{1,0:T(8,128)(2,1)} %param.16) | copy-start | bytes 3145732
  142.9 195.0 %all-gather.20.cloned.1.call-start = ((), (), s32[]{:S(2)}) async-start(), calls=%async_computation.8 | async-start | bytes 10485760 | tf_op jit(solution)/shard_map/all_gather | solution.py:86
  146.9 42.6 %copy-start.3 = (f32[512]{0:T(512)S(1)}, f32[512]{0:T(512)}, u32[]{:S(2)}) copy-start(f32[512]{0:T(512)} %param.31) | copy-start | bytes 6148
  146.9 374.6 %copy-start.6 = (f32[2048]{0:T(1024)S(1)}, f32[2048]{0:T(1024)}, u32[]{:S(2)}) copy-start(f32[2048]{0:T(1024)} %param.29) | copy-start | bytes 24580
  146.9 374.6 %copy-start.7 = (f32[2048]{0:T(1024)S(1)}, f32[2048]{0:T(1024)}, u32[]{:S(2)}) copy-start(f32[2048]{0:T(1024)} %param.27) | copy-start | bytes 24580
  146.9 340.4 %all-gather.22.cloned.1.call-start = ((), (), s32[]{:S(2)}) async-start(), calls=%async_computation.9 | async-start | bytes 10485760 | tf_op jit(solution)/shard_map/all_gather | solution.py:99
  151.4 370.1 %all-gather.18.cloned.1.call-start = ((), (), s32[]{:S(2)}) async-start(), calls=%async_computation.7 | async-start | bytes 5242880 | tf_op jit(solution)/shard_map/all_gather | solution.py:92
  189.5 402.4 %reduce-scatter.5.cloned.1.call-start = ((), (), s32[]{:S(2)}) async-start(), calls=%async_computation.10 | async-start | bytes 5242880 | tf_op jit(solution)/shard_map/reduce_scatter | solution.py:106
  521.6 70.3 %copy-start.1 = (bf16[1024,512]{1,0:T(8,128)(2,1)S(1)}, bf16[1024,512]{1,0:T(8,128)(2,1)}, u32[]{:S(2)}) copy-start(bf16[1024,512]{1,0:T(8,128)(2,1)} %get-tuple-element.10) | copy-start | bytes 3145732
Sparse Core Ops, SparseCore 0:
  8.9 30.8 all-gather.13
  41.3 33.8 all-gather.9
  76.8 27.9 all-gather.11
  106.2 27.3 all-gather.15
  143.1 43.7 reduce-scatter.2
  188.3 149.6 all-gather.19
  339.5 147.7 all-gather.21
  488.9 32.6 all-gather.17
  547.5 44.3 reduce-scatter.4
where the time goes:
time: 601 us
  waiting for transfers between devices  481 us (80%)
  blocking collectives  45.1 us (8%)
  matrix products  40.3 us (7%)
  other arithmetic  20.6 us (3%)
  between operations  13.3 us (2%)
    all_gather x1, waiting for transfers between devices, per_device(): full_down = lax.all_gather(down_rounded, 'fs', axis=1, tiled=True)  149 us
    all_gather x1, waiting for transfers between devices, per_device(): lax.all_gather(weight_up.astype(jnp.bfloat16), 'fs', axis=0, tiled=True)  130 us
    reduce_scatter x2, waiting for transfers between devices, per_device(): lax.psum_scatter((product * piece_scale[:, None]).astype(jnp.bfloat16), '...  79.9 us
    all_gather x1, waiting for transfers between devices, per_device(): lax.all_gather(tokens, 'tp', axis=1, tiled=True).astype(jnp.float32)  35.4 us
    all_gather x1, waiting for transfers between devices, per_device(): lax.all_gather(residual, 'tp', axis=1, tiled=True).astype(jnp.float32)  34.2 us
    all_gather x1, waiting for transfers between devices, per_device(): full_out = lax.all_gather(out_rounded, 'fs', axis=1, tiled=True)  28.8 us
    dot_general x1, matrix products, per_device(): lax.dot_general(columns, hidden, (((0,), (1,)), ((), ())), preferred_elem...  25.7 us
    all_gather x1, waiting for transfers between devices, per_device(): lax.all_gather(weight_u.astype(jnp.bfloat16), 'fs', axis=0, tiled=True)  17.9 us
  transfers between devices with their start and end apart: 9, of which 9 were waited for; matrix products, arithmetic and copies ran while one was open for 4% of the time, Pallas kernels for 0%

commit v1 on v0

v1 whole, which is shorter than its diff:
```python
import jax
import jax.numpy as jnp
from jax import lax
from jax.sharding import PartitionSpec as P

GM_W = 1024
GROUPS = 4
BLOCK = 128


def swap(value, axis, size, mask):
    return lax.ppermute(value, axis, [(k, k ^ mask) for k in range(size)])


def over_fs(piece, fs):
    if fs != 4:
        return [piece] + [swap(piece, "fs", fs, mask) for mask in range(1, fs)]
    far = swap(piece, "fs", 4, 2)
    near = swap(piece, "fs", 4, 1)
    middle = lax.ppermute(piece, "fs", [(1, 2), (2, 1)])
    relayed = lax.ppermute(far, "fs", [(1, 0), (2, 3)])
    me = lax.axis_index("fs")
    last = jnp.where((me == 1) | (me == 2), middle, relayed)
    return [piece, near, far, last]


def gather_weight(shard, cut_axis, fs):
    half = shard.shape[cut_axis] // 2
    group = lax.axis_index("grp")
    mine = lax.dynamic_slice_in_dim(shard, group * half, half, cut_axis)
    other = lax.dynamic_slice_in_dim(shard, (1 - group) * half, half, cut_axis)
    firsts = over_fs(mine, fs)
    seconds = [other] + [
        lax.ppermute(firsts[mask], "grp", [(0, 1), (1, 0)]) for mask in range(1, fs)
    ]
    return firsts, seconds


def halves_swapped(value, axis):
    half = value.shape[axis] // 2
    group = lax.axis_index("grp")
    return jnp.concatenate(
        [
            lax.dynamic_slice_in_dim(value, group * half, half, axis),
            lax.dynamic_slice_in_dim(value, (1 - group) * half, half, axis),
        ],
        axis=axis,
    )


def gather_rows(piece, tp):
    blocks = [None] * tp
    blocks[0] = piece
    bit = tp // 2
    while bit:
        for at in range(tp):
            if blocks[at] is not None and not at & bit and blocks[at | bit] is None:
                blocks[at | bit] = "due"
        for at in range(tp):
            if isinstance(blocks[at], str):
                blocks[at] = swap(blocks[at ^ bit], "tp", tp, bit)
        bit //= 2
    return blocks


def normed_blocks(blocks, gain, fs, tp):
    feature_count = gain.shape[0]
    width, fine = feature_count // tp, feature_count // fs
    squares = sum(
        jnp.sum(jnp.square(block.astype(jnp.float32)), axis=1) for block in blocks
    )
    inverse = lax.rsqrt(squares / feature_count + 1e-06)[:, None]
    stacked = jnp.stack(blocks)
    me_fs, me_tp = lax.axis_index("fs"), lax.axis_index("tp")
    pieces = []
    for mask in range(fs):
        block = me_fs ^ mask
        first = block * fine
        whole = lax.dynamic_index_in_dim(stacked, (first // width) ^ me_tp, 0, keepdims=False)
        if fine != width:
            whole = lax.dynamic_slice_in_dim(whole, first % width, fine, 1)
        gain_piece = lax.dynamic_slice_in_dim(gain, first, fine, 0)
        pieces.append((whole.astype(jnp.float32) * inverse * gain_piece).astype(jnp.bfloat16))
    return jnp.concatenate(pieces, axis=1)


def scatter_sum(terms, fs, tp):
    stacked = jnp.stack(terms)
    ratio = fs // tp
    me_fs, me_tp = lax.axis_index("fs"), lax.axis_index("tp")
    sums = []
    for mask in range(tp):
        parts = [
            lax.dynamic_index_in_dim(
                stacked, ((me_tp ^ mask) * ratio + at) ^ me_fs, 0, keepdims=False
            )
            for at in range(ratio)
        ]
        sums.append(parts[0] if ratio == 1 else jnp.concatenate(parts, axis=1))
    bit = 1
    while bit < tp:
        kept = {}
        for at in range(tp):
            if sums[at] is not None and not at & bit:
                got = swap(sums[at | bit].astype(jnp.bfloat16), "tp", tp, bit)
                kept[at] = sums[at].astype(jnp.float32) + got.astype(jnp.float32)
        sums = [kept.get(at) for at in range(tp)]
        bit *= 2
    return sums[0]


def make(fs, tp):
    def layer(
        tokens,
        norm1_gain,
        weight_u,
        weight_v,
        scale_u,
        scale_v,
        mix_gain,
        spatial_weight,
        spatial_bias,
        weight_out,
        scale_out,
        norm2_gain,
        weight_up,
        scale_up,
        weight_down,
        scale_down,
    ):
        half = weight_u.shape[1] // 2
        token_blocks = gather_rows(tokens, tp)
        both = jnp.stack([weight_u, weight_v], axis=1).astype(jnp.bfloat16)
        both_mine, both_other = gather_weight(both, 2, fs)
        scales = jnp.stack([scale_out, scale_down])
        all_scales = [scales] + [swap(scales, "fs", fs, mask) for mask in range(1, fs)]
        out_mine, out_other = gather_weight(weight_out.astype(jnp.bfloat16), 0, fs)
        up_mine, up_other = gather_weight(weight_up.astype(jnp.bfloat16), 1, fs)
        down_mine, down_other = gather_weight(weight_down.astype(jnp.bfloat16), 0, fs)

        normed_in = normed_blocks(token_blocks, norm1_gain, fs, tp)
        full_u = jnp.concatenate(
            [jnp.concatenate([a[:, 0], b[:, 0]], axis=1) for a, b in zip(both_mine, both_other)]
        )
        full_v = jnp.concatenate(
            [jnp.concatenate([a[:, 1], b[:, 1]], axis=1) for a, b in zip(both_mine, both_other)]
        )
        pre_v = jnp.dot(normed_in, full_v, preferred_element_type=jnp.float32)
        pre_u = jnp.dot(normed_in, full_u, preferred_element_type=jnp.float32)
        act_v = jax.nn.gelu(pre_v * halves_swapped(scale_v, 0))
        gate_u = jax.nn.gelu(pre_u * halves_swapped(scale_u, 0))
        local_width = 2 * half
        row_sums, row_squares = lax.psum(
            (jnp.sum(act_v, axis=1), jnp.sum(act_v * act_v, axis=1)), "tp"
        )
        row_mean = (row_sums / GM_W)[:, None]
        square = (row_squares / GM_W)[:, None]
        v_norm = (
            (act_v - row_mean)
            * lax.rsqrt(square - row_mean * row_mean + 1e-06)
            * halves_swapped(mix_gain, 0)
        ).astype(jnp.bfloat16)
        group_index = lax.axis_index("tp") * local_width // (GM_W // GROUPS)
        lower_mask = jnp.tril(jnp.ones((BLOCK, BLOCK), jnp.float32))
        spatial_mask = (
            lax.dynamic_index_in_dim(spatial_weight, group_index, 0, keepdims=False) * lower_mask
        ).astype(jnp.bfloat16)
        block_bias = lax.dynamic_index_in_dim(spatial_bias, group_index, 0, keepdims=False)
        blocks = v_norm.reshape(-1, BLOCK, local_width)
        mixed = jnp.einsum("ts,nsc->ntc", spatial_mask, blocks, preferred_element_type=jnp.float32)
        mixed = mixed + block_bias[None, :, None]
        gated = (gate_u * mixed.reshape(-1, local_width)).astype(jnp.bfloat16)

        terms = []
        for a, b, scale in zip(out_mine, out_other, all_scales):
            product = jnp.dot(gated, jnp.concatenate([a, b]), preferred_element_type=jnp.float32)
            terms.append((product * scale[0]).astype(jnp.bfloat16))
        mixer_sum = scatter_sum(terms, fs, tp)
        residual = (tokens.astype(jnp.float32) + mixer_sum).astype(jnp.bfloat16)

        normed_mid = normed_blocks(gather_rows(residual, tp), norm2_gain, fs, tp)
        full_up = jnp.concatenate(
            [jnp.concatenate([a, b], axis=1) for a, b in zip(up_mine, up_other)]
        )
        pre_up = jnp.dot(normed_mid, full_up, preferred_element_type=jnp.float32)
        hidden = jnp.square(jax.nn.relu(pre_up * halves_swapped(scale_up, 0))).astype(jnp.bfloat16)
        terms = []
        for a, b, scale in zip(down_mine, down_other, all_scales):
            product = jnp.dot(hidden, jnp.concatenate([a, b]), preferred_element_type=jnp.float32)
            terms.append((product * scale[1]).astype(jnp.bfloat16))
        channel_sum = scatter_sum(terms, fs, tp)
        return (residual.astype(jnp.float32) + channel_sum).astype(jnp.bfloat16)

    return layer


def solution(mesh):
    placed = (
        P(("grp", "fs"), "tp"),
        P(),
        P("fs", "tp"),
        P("fs", "tp"),
        P("tp"),
        P("tp"),
        P("tp"),
        P(),
        P(),
        P("tp", "fs"),
        P("fs"),
        P(),
        P("fs", "tp"),
        P("tp"),
        P("tp", "fs"),
        P("fs"),
    )
    fs, tp = mesh.shape["fs"], mesh.shape["tp"]
    return jax.shard_map(
        make(fs, tp),
        mesh=mesh,
        in_specs=placed,
        out_specs=P(("grp", "fs"), "tp"),
        check_vma=False,
    )
```

time: 601 us -> 439 us (0.73)
  waiting for transfers between devices: 481 us -> 233 us
  starting transfers between devices: 0.33 us -> 90.7 us
  blocking collectives: 45.1 us -> 5.94 us
  matrix products: 40.3 us -> 60.2 us
  local copies, waits for them, and re-layouts: 0.05 us -> 19.3 us
  between operations: 13.3 us -> 0.78 us
  other arithmetic: 20.6 us -> 28.2 us
    all_gather x7 -> x0, waiting for transfers between devices: 400 us -> none  [the longest x1 149 us: per_device(): full_down = lax.all_gather(down_rounded, 'fs', axis=1, tiled=True)]
    ppermute x0 -> x43, waiting for transfers between devices: none -> 233 us  [the longest x23 154 us: swap(): return lax.ppermute(value, axis, [(k, k ^ mask) for k in range(size)])]
    ppermute x0 -> x43, starting transfers between devices: none -> 90.7 us  [the longest x23 67.4 us: swap(): return lax.ppermute(value, axis, [(k, k ^ mask) for k in range(size)])]
    reduce_scatter x2 -> x0, waiting for transfers between devices: 79.9 us -> none  [per_device(): lax.psum_scatter((product * piece_scale[:, None]).astype(jnp.bfloat16), '...]
    all_gather x2 -> x0, blocking collectives: 24.6 us -> none  [the longest x1 12.7 us: per_device(): lax.all_gather(scale_out, 'fs', axis=0, tiled=True)]
    dot_general x4 -> x12, matrix products: 40.3 us -> 60.2 us  [the longest x1 32.6 us: layer(): pre_up = jnp.dot(normed_mid, full_up, preferred_element_type=jnp.float32)]
    psum x3 -> x1, blocking collectives: 20.4 us -> 5.94 us  [layer(): lax.psum((jnp.sum(act_v, axis=1), jnp.sum(act_v * act_v, axis=1)), 'tp')]
    squeeze x0 -> x9, local copies, waits for them, and re-layouts: none -> 9.67 us  [the longest x3 3.95 us: layer(): a[:, 0]]
  transfers between devices with their start and end apart: 9 -> 43, of which waited for: 9 -> 17; matrix products, arithmetic and copies ran while one was open for 4% -> 21% of each run, Pallas kernels for 0% -> 0%
where the time goes in v1:
time: 439 us; the launch traced here: 438 us
  waiting for transfers between devices  233 us (53%)
  starting transfers between devices  90.7 us (21%)
  matrix products  60.2 us (14%)
  other arithmetic  28.2 us (6%)
  local copies, waits for them, and re-layouts  19.3 us (4%)
  blocking collectives  5.94 us (1%)
    ppermute x23, waiting for transfers between devices, swap(): return lax.ppermute(value, axis, [(k, k ^ mask) for k in range(size)])  154 us
    ppermute x12, waiting for transfers between devices, gather_weight(): lax.ppermute(firsts[mask], 'grp', [(0, 1), (1, 0)])  74.5 us
    ppermute x23, starting transfers between devices, swap(): return lax.ppermute(value, axis, [(k, k ^ mask) for k in range(size)])  67.4 us
    dot_general x1, matrix products, layer(): pre_up = jnp.dot(normed_mid, full_up, preferred_element_type=jnp.float32)  32.6 us
    dot_general x4, matrix products, layer(): jnp.dot(hidden, jnp.concatenate([a, b]), preferred_element_type=jnp.float32)  16.5 us
    ppermute x12, starting transfers between devices, gather_weight(): lax.ppermute(firsts[mask], 'grp', [(0, 1), (1, 0)])  13.6 us
  transfers between devices with their start and end apart: 43, of which 17 were waited for; matrix products, arithmetic and copies ran while one was open for 21% of the time, Pallas kernels for 0%

profile of v1, /device:TPU:0, one launch (start us, length us, event | category | flops | bytes accessed | tf_op | source)
XLA Modules:
  0.0 438.4 jit_solution(2556217981708707937)
XLA Ops:
  3.1 4.1 collective-permute-start.5
  8.5 2.2 collective-permute-start.3
  13.2 1.8 slice_bitcast_fusion.14
  21.3 2.0 collective-permute-start.15
  23.9 1.9 collective-permute-done.15
  25.8 3.7 collective-permute-start.19
  32.0 6.8 %collective-permute-done.13 = bf16[128,512]{1,0:T(8,128)(2,1)} collective-permute-done((bf16[128,512]{1,0:T(8,128)(2,1)}, bf16[128,512]{1,0:T(8,128)(2,1)}, u32[]{:S(2)}, u32[]{:S(2)}) %collective-permute-start.13) | collective-permute-done | bytes 131104 | tf_op jit(solution)/shard_map/ppermute | solution.py:12
  40.8 1.6 slice_bitcast_fusion.11
  43.7 1.6 slice_bitcast_fusion.13
  45.4 2.4 collective-permute-done.17
  48.1 1.6 collective-permute-start.6
  49.8 2.5 collective-permute-done.8
  52.2 1.6 collective-permute-start.4
  54.5 3.0 collective-permute-done.6
  57.6 1.6 collective-permute-start.9
  60.3 2.9 collective-permute-done.4
  63.2 1.6 collective-permute-start.11
  65.4 3.4 collective-permute-done.9
  73.7 2.4 fusion.170
  76.2 5.9 %all-reduce = (f32[1024]{0:T(1024)S(1)}, f32[1024]{0:T(1024)S(1)}) all-reduce(f32[1024]{0:T(1024)S(1)} %get-tuple-element.6, f32[1024]{0:T(1024)S(1)} %get-tuple-element.5), channel_id=1, replica_groups=mesh['grp'=2,'fs'=4,'tp'=4] {'tp'}, use_global_device_ids=true, to_apply=%region_7.8 | all-reduce | flops 2048 | bytes 16384 | tf_op jit(solution)/shard_map/psum | solution.py:153
  82.2 1.7 multiply_convert_fusion.9
  85.1 2.7 fusion.99
  93.4 1.7 dynamic-slice_bitcast_fusion.3
  96.0 2.5 convert_element_type.251
  100.1 2.7 collective-permute-start.28
  103.0 3.0 fusion.57
  106.0 1.8 collective-permute-start.22
  107.8 2.5 convert_element_type.253
  110.7 1.6 collective-permute-start.30
  112.4 59.9 %collective-permute-done.28 = bf16[512,1024]{1,0:T(8,128)(2,1)} collective-permute-done((bf16[512,1024]{1,0:T(8,128)(2,1)}, bf16[512,1024]{1,0:T(8,128)(2,1)}, u32[]{:S(2)}, u32[]{:S(2)}) %collective-permute-start.28) | collective-permute-done | bytes 1048608 | tf_op jit(solution)/shard_map/ppermute | solution.py:12
  174.3 2.8 fusion.29
  177.1 1.8 collective-permute-start.24
  178.9 15.8 %collective-permute-done.35 = bf16[1024,512]{1,0:T(8,128)(2,1)} collective-permute-done((bf16[1024,512]{1,0:T(8,128)(2,1)S(1)}, bf16[1024,512]{1,0:T(8,128)(2,1)}, u32[]{:S(2)}, u32[]{:S(2)}) %collective-permute-start.35) | collective-permute-done | bytes 1048608 | tf_op jit(solution)/shard_map/ppermute | solution.py:12
  196.3 21.5 %collective-permute-start.26 = (bf16[512,1024]{1,0:T(8,128)(2,1)}, bf16[512,1024]{1,0:T(8,128)(2,1)S(1)}, u32[]{:S(2)}, u32[]{:S(2)}) collective-permute-start(bf16[512,1024]{1,0:T(8,128)(2,1)} %get-tuple-element.26), channel_id=1, source_target_pairs={{0,4},{4,0},{8,12},{12,8},{1,5},{5,1},{9,13},{13,9},{2,6},{6,2},{1... | collective-permute-start | bytes 3145736 | tf_op jit(solution)/shard_map/ppermute | solution.py:12
  217.8 22.0 %collective-permute-start.33 = (bf16[1024,512]{1,0:T(8,128)(2,1)S(1)}, bf16[1024,512]{1,0:T(8,128)(2,1)}, u32[]{:S(2)}, u32[]{:S(2)}) collective-permute-start(bf16[1024,512]{1,0:T(8,128)(2,1)S(1)} %get-tuple-element.24), channel_id=1, source_target_pairs={{0,4},{4,0},{8,12},{12,8},{1,5},{5,1},{9,13},{13,9},{2,6},{6,2},{1... | collective-permute-start | bytes 3145736 | tf_op jit(solution)/shard_map/ppermute | solution.py:12
  242.6 19.1 %collective-permute-done.26 = bf16[512,1024]{1,0:T(8,128)(2,1)S(1)} collective-permute-done((bf16[512,1024]{1,0:T(8,128)(2,1)}, bf16[512,1024]{1,0:T(8,128)(2,1)S(1)}, u32[]{:S(2)}, u32[]{:S(2)}) %collective-permute-start.26) | collective-permute-done | bytes 1048608 | tf_op jit(solution)/shard_map/ppermute | solution.py:12
  262.3 22.0 %collective-permute-done.33 = bf16[1024,512]{1,0:T(8,128)(2,1)} collective-permute-done((bf16[1024,512]{1,0:T(8,128)(2,1)S(1)}, bf16[1024,512]{1,0:T(8,128)(2,1)}, u32[]{:S(2)}, u32[]{:S(2)}) %collective-permute-start.33) | collective-permute-done | bytes 1048608 | tf_op jit(solution)/shard_map/ppermute | solution.py:12
  288.0 2.1 fusion.56
  291.6 20.3 %collective-permute-done.27 = bf16[512,1024]{1,0:T(8,128)(2,1)S(1)} collective-permute-done((bf16[512,1024]{1,0:T(8,128)(2,1)S(1)}, bf16[512,1024]{1,0:T(8,128)(2,1)S(1)}, u32[]{:S(2)}, u32[]{:S(2)}) %collective-permute-start.27) | collective-permute-done | bytes 1048608 | tf_op jit(solution)/shard_map/ppermute | solution.py:34
  311.9 44.9 %collective-permute-done.32 = bf16[512,1024]{1,0:T(8,128)(2,1)S(1)} collective-permute-done((bf16[512,1024]{1,0:T(8,128)(2,1)S(1)}, bf16[512,1024]{1,0:T(8,128)(2,1)S(1)}, u32[]{:S(2)}, u32[]{:S(2)}) %collective-permute-start.32) | collective-permute-done | bytes 1048608 | tf_op jit(solution)/shard_map/ppermute | solution.py:34
  357.8 32.6 %multiply_convert_fusion = bf16[1024,2048]{1,0:T(8,128)(2,1)} fusion(f32[2048]{0:T(1024)S(1)} %pad_maximum_fusion.7, bf16[512,1024]{1,0:T(8,128)(2,1)} %copy-done.37, bf16[512,1024]{1,0:T(8,128)(2,1)} %copy-done.9, bf16[512,1024]{1,0:T(8,128)(2,1)} %copy-done.35, bf16[512,1024]{1,0:T(8,128)(2,1)} %collective-permute-done.28, ...), kind=kOutput, calls=%fused_computation.16 | convolution fusion | flops 8682209280 | bytes 16785408 | tf_op jit(solution)/shard_map/dot_general | solution.py:185
  390.4 4.8 %fusion.79 = bf16[1,1024,512]{1,2,0:T(8,128)(2,1)S(1)} fusion(bf16[1024,2048]{1,0:T(8,128)(2,1)} %multiply_convert_fusion, bf16[1024,512]{1,0:T(8,128)(2,1)S(1)} %get-tuple-element.23, bf16[1024,512]{1,0:T(8,128)(2,1)S(1)} %get-tuple-element.24, f32[512]{0:T(512)S(1)} %copy-done.25), kind=kOutput, calls=%fused_computation.105 | convolution fusion | flops 2152726528 | bytes 7342080 | tf_op jit(solution)/shard_map/dot_general | solution.py:189
  395.2 3.9 fusion.82
  399.1 3.9 fusion.85
  403.0 3.9 fusion.88
  408.3 2.1 collective-permute-done.41
  410.9 1.8 collective-permute-start.42
  412.7 23.5 %collective-permute-done.42 = bf16[1024,512]{0,1:T(8,128)(2,1)S(1)} collective-permute-done((bf16[1024,512]{0,1:T(8,128)(2,1)S(1)}, bf16[1024,512]{0,1:T(8,128)(2,1)S(1)}, u32[]{:S(2)}, u32[]{:S(2)}) %collective-permute-start.42) | collective-permute-done | bytes 1048608 | tf_op jit(solution)/shard_map/ppermute | solution.py:12
  (188 shorter events, 54.0 us)
Async XLA Ops:
  3.1 36.4 %collective-permute-start.5 = (bf16[512,2,128]{2,0,1:T(8,128)(2,1)S(1)}, bf16[512,2,128]{2,0,1:T(8,128)(2,1)}, u32[]{:S(2)}, u32[]{:S(2)}) collective-permute-start(bf16[512,2,128]{2,0,1:T(8,128)(2,1)S(1)} %get-tuple-element.28), channel_id=1, source_target_pairs={{0,8},{4,12},{8,0},{12,4},{1,9},{5,13},{9,1},{13,5},{2,10},{6,14},... | collective-permute-start | bytes 786440 | tf_op jit(solution)/shard_map/ppermute | solution.py:12
  7.1 41.0 %collective-permute-start.7 = (bf16[512,2,128]{2,0,1:T(8,128)(2,1)S(1)}, bf16[512,2,128]{2,0,1:T(8,128)(2,1)}, u32[]{:S(2)}, u32[]{:S(2)}) collective-permute-start(bf16[512,2,128]{2,0,1:T(8,128)(2,1)S(1)} %get-tuple-element.28), channel_id=1, source_target_pairs={{4,8},{8,4},{5,9},{9,5},{6,10},{10,6},{7,11},{11,7},{20,24},{24,20... | collective-permute-start | bytes 786440 | tf_op jit(solution)/shard_map/ppermute | solution.py:20
  8.5 33.9 %collective-permute-start.3 = (bf16[512,2,128]{2,0,1:T(8,128)(2,1)S(1)}, bf16[512,2,128]{2,0,1:T(8,128)(2,1)}, u32[]{:S(2)}, u32[]{:S(2)}) collective-permute-start(bf16[512,2,128]{2,0,1:T(8,128)(2,1)S(1)} %get-tuple-element.28), channel_id=1, source_target_pairs={{0,4},{4,0},{8,12},{12,8},{1,5},{5,1},{9,13},{13,9},{2,6},{6,2},{1... | collective-permute-start | bytes 786440 | tf_op jit(solution)/shard_map/ppermute | solution.py:12
  10.7 48.5 %collective-permute-start.1 = (bf16[1024,512]{1,0:T(8,128)(2,1)S(1)}, bf16[1024,512]{1,0:T(8,128)(2,1)S(1)}, u32[]{:S(2)}, u32[]{:S(2)}) collective-permute-start(bf16[1024,512]{1,0:T(8,128)(2,1)S(1)} %copy-done.3), channel_id=1, source_target_pairs={{0,2},{1,3},{2,0},{3,1},{4,6},{5,7},{6,4},{7,5},{8,10},{9,11},{10,... | collective-permute-start | bytes 3145736 | tf_op jit(solution)/shard_map/ppermute | solution.py:12
  12.2 9.1 %collective-permute-start.12 = (f32[2,512]{1,0:T(2,128)S(1)}, f32[2,512]{1,0:T(2,128)S(1)}, u32[]{:S(2)}, u32[]{:S(2)}) collective-permute-start(f32[2,512]{1,0:T(2,128)S(1)} %pad_maximum_fusion.8), channel_id=1, source_target_pairs={{0,4},{4,0},{8,12},{12,8},{1,5},{5,1},{9,13},{13,9},{2,6},{6,2},{1... | collective-permute-start | bytes 12296 | tf_op jit(solution)/shard_map/ppermute | solution.py:12
  21.3 4.5 %collective-permute-start.15 = (f32[2,512]{1,0:T(2,128)S(1)}, f32[2,512]{1,0:T(2,128)S(1)}, u32[]{:S(2)}, u32[]{:S(2)}) collective-permute-start(f32[2,512]{1,0:T(2,128)S(1)} %pad_maximum_fusion.8), channel_id=1, source_target_pairs={{0,8},{4,12},{8,0},{12,4},{1,9},{5,13},{9,1},{13,5},{2,10},{6,14},... | collective-permute-start | bytes 12296 | tf_op jit(solution)/shard_map/ppermute | solution.py:12
  25.8 5.4 %collective-permute-start.19 = (f32[2,512]{1,0:T(2,128)S(1)}, f32[2,512]{1,0:T(2,128)S(1)}, u32[]{:S(2)}, u32[]{:S(2)}) collective-permute-start(f32[2,512]{1,0:T(2,128)S(1)} %pad_maximum_fusion.8), channel_id=1, source_target_pairs={{0,12},{4,8},{8,4},{12,0},{1,13},{5,9},{9,5},{13,1},{2,14},{6,10},... | collective-permute-start | bytes 12296 | tf_op jit(solution)/shard_map/ppermute | solution.py:12
  31.2 7.6 %collective-permute-start.13 = (bf16[128,512]{1,0:T(8,128)(2,1)}, bf16[128,512]{1,0:T(8,128)(2,1)}, u32[]{:S(2)}, u32[]{:S(2)}) collective-permute-start(bf16[128,512]{1,0:T(8,128)(2,1)} %get-tuple-element.30), channel_id=1, source_target_pairs={{0,8},{4,12},{8,0},{12,4},{1,9},{5,13},{9,1},{13,5},{2,10},{6,14},... | collective-permute-start | bytes 393224 | tf_op jit(solution)/shard_map/ppermute | solution.py:12
  38.8 6.5 %collective-permute-start.16 = (bf16[128,512]{1,0:T(8,128)(2,1)}, bf16[128,512]{1,0:T(8,128)(2,1)S(1)}, u32[]{:S(2)}, u32[]{:S(2)}) collective-permute-start(bf16[128,512]{1,0:T(8,128)(2,1)} %get-tuple-element.30), channel_id=1, source_target_pairs={{4,8},{8,4},{5,9},{9,5},{6,10},{10,6},{7,11},{11,7},{20,24},{24,20... | collective-permute-start | bytes 393224 | tf_op jit(solution)/shard_map/ppermute | solution.py:20
  39.5 8.3 %collective-permute-start.17 = (bf16[128,512]{1,0:T(8,128)(2,1)}, bf16[128,512]{1,0:T(8,128)(2,1)S(1)}, u32[]{:S(2)}, u32[]{:S(2)}) collective-permute-start(bf16[128,512]{1,0:T(8,128)(2,1)} %collective-permute-done.13), channel_id=1, source_target_pairs={{4,0},{8,12},{5,1},{9,13},{6,2},{10,14},{7,3},{11,15},{20,16},{24,... | collective-permute-start | bytes 393224 | tf_op jit(solution)/shard_map/ppermute | solution.py:21
  42.4 9.8 %collective-permute-start.8 = (bf16[512,2,128]{2,0,1:T(8,128)(2,1)}, bf16[512,2,128]{2,0,1:T(8,128)(2,1)S(1)}, u32[]{:S(2)}, u32[]{:S(2)}) collective-permute-start(bf16[512,2,128]{2,0,1:T(8,128)(2,1)} %collective-permute-done.5), channel_id=1, source_target_pairs={{4,0},{8,12},{5,1},{9,13},{6,2},{10,14},{7,3},{11,15},{20,16},{24,... | collective-permute-start | bytes 786440 | tf_op jit(solution)/shard_map/ppermute | solution.py:21
  45.4 26.0 %collective-permute-start = (bf16[1024,512]{1,0:T(8,128)(2,1)S(1)}, bf16[1024,512]{1,0:T(8,128)(2,1)S(1)}, u32[]{:S(2)}, u32[]{:S(2)}) collective-permute-start(bf16[1024,512]{1,0:T(8,128)(2,1)S(1)} %copy-done.3), channel_id=1, source_target_pairs={{0,1},{1,0},{2,3},{3,2},{4,5},{5,4},{6,7},{7,6},{8,9},{9,8},{10,11... | collective-permute-start | bytes 3145736 | tf_op jit(solution)/shard_map/ppermute | solution.py:12
  47.8 12.1 %collective-permute-start.10 = (bf16[128,512]{1,0:T(8,128)(2,1)}, bf16[128,512]{1,0:T(8,128)(2,1)}, u32[]{:S(2)}, u32[]{:S(2)}) collective-permute-start(bf16[128,512]{1,0:T(8,128)(2,1)} %get-tuple-element.30), channel_id=1, source_target_pairs={{0,4},{4,0},{8,12},{12,8},{1,5},{5,1},{9,13},{13,9},{2,6},{6,2},{1... | collective-permute-start | bytes 393224 | tf_op jit(solution)/shard_map/ppermute | solution.py:12
  48.1 9.5 %collective-permute-start.6 = (bf16[512,2,128]{2,0,1:T(8,128)(2,1)}, bf16[512,2,128]{2,0,1:T(8,128)(2,1)S(1)}, u32[]{:S(2)}, u32[]{:S(2)}) collective-permute-start(bf16[512,2,128]{2,0,1:T(8,128)(2,1)} %collective-permute-done.5), channel_id=1, source_target_pairs={{0,16},{16,0},{1,17},{17,1},{2,18},{18,2},{3,19},{19,3},{4,20},{20... | collective-permute-start | bytes 786440 | tf_op jit(solution)/shard_map/ppermute | solution.py:34
  52.2 11.0 %collective-permute-start.4 = (bf16[512,2,128]{2,0,1:T(8,128)(2,1)}, bf16[512,2,128]{2,0,1:T(8,128)(2,1)S(1)}, u32[]{:S(2)}, u32[]{:S(2)}) collective-permute-start(bf16[512,2,128]{2,0,1:T(8,128)(2,1)} %collective-permute-done.3), channel_id=1, source_target_pairs={{0,16},{16,0},{1,17},{17,1},{2,18},{18,2},{3,19},{19,3},{4,20},{20... | collective-permute-start | bytes 786440 | tf_op jit(solution)/shard_map/ppermute | solution.py:34
  57.6 11.2 %collective-permute-start.9 = (bf16[512,2,128]{2,0,1:T(8,128)(2,1)S(1)}, bf16[512,2,128]{2,0,1:T(8,128)(2,1)S(1)}, u32[]{:S(2)}, u32[]{:S(2)}) collective-permute-start(bf16[512,2,128]{2,0,1:T(8,128)(2,1)S(1)} %broadcast_select_fusion.2), channel_id=1, source_target_pairs={{0,16},{16,0},{1,17},{17,1},{2,18},{18,2},{3,19},{19,3},{4,20},{20... | collective-permute-start | bytes 786440 | tf_op jit(solution)/shard_map/ppermute | solution.py:34
  59.1 12.5 %collective-permute-start.2 = (bf16[1024,512]{1,0:T(8,128)(2,1)S(1)}, bf16[1024,512]{1,0:T(8,128)(2,1)S(1)}, u32[]{:S(2)}, u32[]{:S(2)}) collective-permute-start(bf16[1024,512]{1,0:T(8,128)(2,1)S(1)} %collective-permute-done.1), channel_id=1, source_target_pairs={{0,1},{1,0},{2,3},{3,2},{4,5},{5,4},{6,7},{7,6},{8,9},{9,8},{10,11... | collective-permute-start | bytes 3145736 | tf_op jit(solution)/shard_map/ppermute | solution.py:12
  59.8 30.9 %collective-permute-start.14 = (bf16[128,512]{1,0:T(8,128)(2,1)}, bf16[128,512]{1,0:T(8,128)(2,1)}, u32[]{:S(2)}, u32[]{:S(2)}) collective-permute-start(bf16[128,512]{1,0:T(8,128)(2,1)} %collective-permute-done.13), channel_id=1, source_target_pairs={{0,16},{16,0},{1,17},{17,1},{2,18},{18,2},{3,19},{19,3},{4,20},{20... | collective-permute-start | bytes 393224 | tf_op jit(solution)/shard_map/ppermute | solution.py:34
  63.2 26.1 %collective-permute-start.11 = (bf16[128,512]{1,0:T(8,128)(2,1)}, bf16[128,512]{1,0:T(8,128)(2,1)}, u32[]{:S(2)}, u32[]{:S(2)}) collective-permute-start(bf16[128,512]{1,0:T(8,128)(2,1)} %collective-permute-done.10), channel_id=1, source_target_pairs={{0,16},{16,0},{1,17},{17,1},{2,18},{18,2},{3,19},{19,3},{4,20},{20... | collective-permute-start | bytes 393224 | tf_op jit(solution)/shard_map/ppermute | solution.py:34
  68.8 23.4 %collective-permute-start.18 = (bf16[128,512]{1,0:T(8,128)(2,1)S(1)}, bf16[128,512]{1,0:T(8,128)(2,1)S(1)}, u32[]{:S(2)}, u32[]{:S(2)}) collective-permute-start(bf16[128,512]{1,0:T(8,128)(2,1)S(1)} %broadcast_select_fusion.3), channel_id=1, source_target_pairs={{0,16},{16,0},{1,17},{17,1},{2,18},{18,2},{3,19},{19,3},{4,20},{20... | collective-permute-start | bytes 393224 | tf_op jit(solution)/shard_map/ppermute | solution.py:34
  96.0 7.0 %collective-permute-start.21 = (bf16[1024,512]{0,1:T(8,128)(2,1)}, bf16[1024,512]{0,1:T(8,128)(2,1)}, u32[]{:S(2)}, u32[]{:S(2)}) collective-permute-start(bf16[1024,512]{0,1:T(8,128)(2,1)} %get-tuple-element.22), channel_id=1, source_target_pairs={{0,1},{1,0},{2,3},{3,2},{4,5},{5,4},{6,7},{7,6},{8,9},{9,8},{10,11... | collective-permute-start | bytes 3145736 | tf_op jit(solution)/shard_map/ppermute | solution.py:12
  100.1 72.2 %collective-permute-start.28 = (bf16[512,1024]{1,0:T(8,128)(2,1)}, bf16[512,1024]{1,0:T(8,128)(2,1)}, u32[]{:S(2)}, u32[]{:S(2)}) collective-permute-start(bf16[512,1024]{1,0:T(8,128)(2,1)} %get-tuple-element.26), channel_id=1, source_target_pairs={{0,8},{4,12},{8,0},{12,4},{1,9},{5,13},{9,1},{13,5},{2,10},{6,14},... | collective-permute-start | bytes 3145736 | tf_op jit(solution)/shard_map/ppermute | solution.py:12
  102.8 70.2 %collective-permute-start.20 = (bf16[1024,512]{0,1:T(8,128)(2,1)}, bf16[1024,512]{0,1:T(8,128)(2,1)}, u32[]{:S(2)}, u32[]{:S(2)}) collective-permute-start(bf16[1024,512]{0,1:T(8,128)(2,1)} %get-tuple-element.21), channel_id=1, source_target_pairs={{0,1},{1,0},{2,3},{3,2},{4,5},{5,4},{6,7},{7,6},{8,9},{9,8},{10,11... | collective-permute-start | bytes 3145736 | tf_op jit(solution)/shard_map/ppermute | solution.py:12
  106.0 68.3 %collective-permute-start.22 = (bf16[1024,512]{0,1:T(8,128)(2,1)}, bf16[1024,512]{0,1:T(8,128)(2,1)}, u32[]{:S(2)}, u32[]{:S(2)}) collective-permute-start(bf16[1024,512]{0,1:T(8,128)(2,1)} %fusion.57), channel_id=1, source_target_pairs={{0,2},{1,3},{2,0},{3,1},{4,6},{5,7},{6,4},{7,5},{8,10},{9,11},{10,... | collective-permute-start | bytes 3145736 | tf_op jit(solution)/shard_map/ppermute | solution.py:12
  110.4 84.4 %collective-permute-start.35 = (bf16[1024,512]{1,0:T(8,128)(2,1)S(1)}, bf16[1024,512]{1,0:T(8,128)(2,1)}, u32[]{:S(2)}, u32[]{:S(2)}) collective-permute-start(bf16[1024,512]{1,0:T(8,128)(2,1)S(1)} %get-tuple-element.24), channel_id=1, source_target_pairs={{0,8},{4,12},{8,0},{12,4},{1,9},{5,13},{9,1},{13,5},{2,10},{6,14},... | collective-permute-start | bytes 3145736 | tf_op jit(solution)/shard_map/ppermute | solution.py:12
  110.7 85.5 %collective-permute-start.30 = (bf16[512,1024]{1,0:T(8,128)(2,1)}, bf16[512,1024]{1,0:T(8,128)(2,1)}, u32[]{:S(2)}, u32[]{:S(2)}) collective-permute-start(bf16[512,1024]{1,0:T(8,128)(2,1)} %get-tuple-element.26), channel_id=1, source_target_pairs={{4,8},{8,4},{5,9},{9,5},{6,10},{10,6},{7,11},{11,7},{20,24},{24,20... | collective-permute-start | bytes 3145736 | tf_op jit(solution)/shard_map/ppermute | solution.py:20
  112.4 127.4 %copy-start.16 = (f32[2048]{0:T(1024)S(1)}, f32[2048]{0:T(1024)}, u32[]{:S(2)}) copy-start(f32[2048]{0:T(1024)} %param.27) | copy-start | bytes 24580
  112.4 127.5 %copy-start.17 = (f32[2048]{0:T(1024)S(1)}, f32[2048]{0:T(1024)}, u32[]{:S(2)}) copy-start(f32[2048]{0:T(1024)} %param.29) | copy-start | bytes 24580
  172.3 45.6 %collective-permute-start.37 = (bf16[1024,512]{1,0:T(8,128)(2,1)S(1)}, bf16[1024,512]{1,0:T(8,128)(2,1)S(1)}, u32[]{:S(2)}, u32[]{:S(2)}) collective-permute-start(bf16[1024,512]{1,0:T(8,128)(2,1)S(1)} %get-tuple-element.24), channel_id=1, source_target_pairs={{4,8},{8,4},{5,9},{9,5},{6,10},{10,6},{7,11},{11,7},{20,24},{24,20... | collective-permute-start | bytes 3145736 | tf_op jit(solution)/shard_map/ppermute | solution.py:20
  173.0 66.8 %collective-permute-start.31 = (bf16[512,1024]{1,0:T(8,128)(2,1)}, bf16[512,1024]{1,0:T(8,128)(2,1)S(1)}, u32[]{:S(2)}, u32[]{:S(2)}) collective-permute-start(bf16[512,1024]{1,0:T(8,128)(2,1)} %collective-permute-done.28), channel_id=1, source_target_pairs={{4,0},{8,12},{5,1},{9,13},{6,2},{10,14},{7,3},{11,15},{20,16},{24,... | collective-permute-start | bytes 3145736 | tf_op jit(solution)/shard_map/ppermute | solution.py:21
  177.1 62.8 %collective-permute-start.24 = (bf16[1024,512]{0,1:T(8,128)(2,1)S(1)}, bf16[1024,512]{0,1:T(8,128)(2,1)S(1)}, u32[]{:S(2)}, u32[]{:S(2)}) collective-permute-start(bf16[1024,512]{0,1:T(8,128)(2,1)S(1)} %get-tuple-element.10), channel_id=1, source_target_pairs={{0,2},{1,3},{2,0},{3,1},{4,6},{5,7},{6,4},{7,5},{8,10},{9,11},{10,... | collective-permute-start | bytes 3145736 | tf_op jit(solution)/shard_map/ppermute | solution.py:12
  194.8 45.8 %collective-permute-start.38 = (bf16[1024,512]{1,0:T(8,128)(2,1)}, bf16[1024,512]{1,0:T(8,128)(2,1)S(1)}, u32[]{:S(2)}, u32[]{:S(2)}) collective-permute-start(bf16[1024,512]{1,0:T(8,128)(2,1)} %collective-permute-done.35), channel_id=1, source_target_pairs={{4,0},{8,12},{5,1},{9,13},{6,2},{10,14},{7,3},{11,15},{20,16},{24,... | collective-permute-start | bytes 3145736 | tf_op jit(solution)/shard_map/ppermute | solution.py:21
  196.3 65.5 %collective-permute-start.26 = (bf16[512,1024]{1,0:T(8,128)(2,1)}, bf16[512,1024]{1,0:T(8,128)(2,1)S(1)}, u32[]{:S(2)}, u32[]{:S(2)}) collective-permute-start(bf16[512,1024]{1,0:T(8,128)(2,1)} %get-tuple-element.26), channel_id=1, source_target_pairs={{0,4},{4,0},{8,12},{12,8},{1,5},{5,1},{9,13},{13,9},{2,6},{6,2},{1... | collective-permute-start | bytes 3145736 | tf_op jit(solution)/shard_map/ppermute | solution.py:12
  217.8 66.4 %collective-permute-start.33 = (bf16[1024,512]{1,0:T(8,128)(2,1)S(1)}, bf16[1024,512]{1,0:T(8,128)(2,1)}, u32[]{:S(2)}, u32[]{:S(2)}) collective-permute-start(bf16[1024,512]{1,0:T(8,128)(2,1)S(1)} %get-tuple-element.24), channel_id=1, source_target_pairs={{0,4},{4,0},{8,12},{12,8},{1,5},{5,1},{9,13},{13,9},{2,6},{6,2},{1... | collective-permute-start | bytes 3145736 | tf_op jit(solution)/shard_map/ppermute | solution.py:12
  239.8 44.9 %collective-permute-start.23 = (bf16[1024,512]{0,1:T(8,128)(2,1)S(1)}, bf16[1024,512]{0,1:T(8,128)(2,1)S(1)}, u32[]{:S(2)}, u32[]{:S(2)}) collective-permute-start(bf16[1024,512]{0,1:T(8,128)(2,1)S(1)} %get-tuple-element.10), channel_id=1, source_target_pairs={{0,1},{1,0},{2,3},{3,2},{4,5},{5,4},{6,7},{7,6},{8,9},{9,8},{10,11... | collective-permute-start | bytes 3145736 | tf_op jit(solution)/shard_map/ppermute | solution.py:12
  239.9 46.6 %collective-permute-start.25 = (bf16[1024,512]{0,1:T(8,128)(2,1)S(1)}, bf16[1024,512]{0,1:T(8,128)(2,1)S(1)}, u32[]{:S(2)}, u32[]{:S(2)}) collective-permute-start(bf16[1024,512]{0,1:T(8,128)(2,1)S(1)} %collective-permute-done.24), channel_id=1, source_target_pairs={{0,1},{1,0},{2,3},{3,2},{4,5},{5,4},{6,7},{7,6},{8,9},{9,8},{10,11... | collective-permute-start | bytes 3145736 | tf_op jit(solution)/shard_map/ppermute | solution.py:12
  240.6 45.9 %copy-start.9 = (bf16[512,1024]{1,0:T(8,128)(2,1)}, bf16[512,1024]{1,0:T(8,128)(2,1)S(1)}, u32[]{:S(2)}) copy-start(bf16[512,1024]{1,0:T(8,128)(2,1)S(1)} %broadcast_select_fusion.1) | copy-start | bytes 3145732
  240.6 49.4 %collective-permute-start.29 = (bf16[512,1024]{1,0:T(8,128)(2,1)}, bf16[512,1024]{1,0:T(8,128)(2,1)S(1)}, u32[]{:S(2)}, u32[]{:S(2)}) collective-permute-start(bf16[512,1024]{1,0:T(8,128)(2,1)} %collective-permute-done.28), channel_id=1, source_target_pairs={{0,16},{16,0},{1,17},{17,1},{2,18},{18,2},{3,19},{19,3},{4,20},{20... | collective-permute-start | bytes 3145736 | tf_op jit(solution)/shard_map/ppermute | solution.py:34
  261.8 137.3 %collective-permute-start.36 = (bf16[1024,512]{1,0:T(8,128)(2,1)}, bf16[1024,512]{1,0:T(8,128)(2,1)}, u32[]{:S(2)}, u32[]{:S(2)}) collective-permute-start(bf16[1024,512]{1,0:T(8,128)(2,1)} %collective-permute-done.35), channel_id=1, source_target_pairs={{0,16},{16,0},{1,17},{17,1},{2,18},{18,2},{3,19},{19,3},{4,20},{20... | collective-permute-start | bytes 3145736 | tf_op jit(solution)/shard_map/ppermute | solution.py:34
  284.2 27.6 %collective-permute-start.27 = (bf16[512,1024]{1,0:T(8,128)(2,1)S(1)}, bf16[512,1024]{1,0:T(8,128)(2,1)S(1)}, u32[]{:S(2)}, u32[]{:S(2)}) collective-permute-start(bf16[512,1024]{1,0:T(8,128)(2,1)S(1)} %collective-permute-done.26), channel_id=1, source_target_pairs={{0,16},{16,0},{1,17},{17,1},{2,18},{18,2},{3,19},{19,3},{4,20},{20... | collective-permute-start | bytes 3145736 | tf_op jit(solution)/shard_map/ppermute | solution.py:34
  284.7 110.4 %collective-permute-start.34 = (bf16[1024,512]{1,0:T(8,128)(2,1)}, bf16[1024,512]{1,0:T(8,128)(2,1)}, u32[]{:S(2)}, u32[]{:S(2)}) collective-permute-start(bf16[1024,512]{1,0:T(8,128)(2,1)} %collective-permute-done.33), channel_id=1, source_target_pairs={{0,16},{16,0},{1,17},{17,1},{2,18},{18,2},{3,19},{19,3},{4,20},{20... | collective-permute-start | bytes 3145736 | tf_op jit(solution)/shard_map/ppermute | solution.py:34
  286.5 70.3 %collective-permute-start.32 = (bf16[512,1024]{1,0:T(8,128)(2,1)S(1)}, bf16[512,1024]{1,0:T(8,128)(2,1)S(1)}, u32[]{:S(2)}, u32[]{:S(2)}) collective-permute-start(bf16[512,1024]{1,0:T(8,128)(2,1)S(1)} %broadcast_select_fusion.1), channel_id=1, source_target_pairs={{0,16},{16,0},{1,17},{17,1},{2,18},{18,2},{3,19},{19,3},{4,20},{20... | collective-permute-start | bytes 3145736 | tf_op jit(solution)/shard_map/ppermute | solution.py:34
  288.0 69.8 %copy-start.4 = (bf16[512,1024]{1,0:T(8,128)(2,1)S(1)}, bf16[512,1024]{1,0:T(8,128)(2,1)}, u32[]{:S(2)}) copy-start(bf16[512,1024]{1,0:T(8,128)(2,1)} %get-tuple-element.25) | copy-start | bytes 3145732
  290.1 66.7 %copy-start.35 = (bf16[512,1024]{1,0:T(8,128)(2,1)}, bf16[512,1024]{1,0:T(8,128)(2,1)S(1)}, u32[]{:S(2)}) copy-start(bf16[512,1024]{1,0:T(8,128)(2,1)S(1)} %collective-permute-done.29) | copy-start | bytes 3145732
  290.1 113.0 %collective-permute-start.39 = (bf16[1024,512]{1,0:T(8,128)(2,1)}, bf16[1024,512]{1,0:T(8,128)(2,1)}, u32[]{:S(2)}, u32[]{:S(2)}) collective-permute-start(bf16[1024,512]{1,0:T(8,128)(2,1)} %broadcast_select_fusion), channel_id=1, source_target_pairs={{0,16},{16,0},{1,17},{17,1},{2,18},{18,2},{3,19},{19,3},{4,20},{20... | collective-permute-start | bytes 3145736 | tf_op jit(solution)/shard_map/ppermute | solution.py:34
  407.7 2.7 collective-permute-start.41
  407.8 4.9 %collective-permute-start.40 = (bf16[1024,512]{0,1:T(8,128)(2,1)S(1)}, bf16[1024,512]{0,1:T(8,128)(2,1)S(1)}, u32[]{:S(2)}, u32[]{:S(2)}) collective-permute-start(bf16[1024,512]{0,1:T(8,128)(2,1)S(1)} %get-tuple-element.19), channel_id=1, source_target_pairs={{0,1},{1,0},{2,3},{3,2},{4,5},{5,4},{6,7},{7,6},{8,9},{9,8},{10,11... | collective-permute-start | bytes 3145736 | tf_op jit(solution)/shard_map/ppermute | solution.py:12
  410.9 25.3 %collective-permute-start.42 = (bf16[1024,512]{0,1:T(8,128)(2,1)S(1)}, bf16[1024,512]{0,1:T(8,128)(2,1)S(1)}, u32[]{:S(2)}, u32[]{:S(2)}) collective-permute-start(bf16[1024,512]{0,1:T(8,128)(2,1)S(1)} %fusion.47), channel_id=1, source_target_pairs={{0,2},{1,3},{2,0},{3,1},{4,6},{5,7},{6,4},{7,5},{8,10},{9,11},{10,... | collective-permute-start | bytes 3145736 | tf_op jit(solution)/shard_map/ppermute | solution.py:12
  (34 other events, 246.7 us)

commit v2 on v1

--- a/solution.py
+++ b/solution.py
@@ -12,8 +12,8 @@
     return lax.ppermute(value, axis, [(k, k ^ mask) for k in range(size)])
 
 
-def over_fs(piece, fs):
-    if fs != 4:
+def over_fs(piece, fs, relay):
+    if fs != 4 or not relay:
         return [piece] + [swap(piece, "fs", fs, mask) for mask in range(1, fs)]
     far = swap(piece, "fs", 4, 2)
     near = swap(piece, "fs", 4, 1)
@@ -24,12 +24,12 @@
     return [piece, near, far, last]
 
 
-def gather_weight(shard, cut_axis, fs):
+def gather_weight(shard, cut_axis, fs, relay=False):
     half = shard.shape[cut_axis] // 2
     group = lax.axis_index("grp")
     mine = lax.dynamic_slice_in_dim(shard, group * half, half, cut_axis)
     other = lax.dynamic_slice_in_dim(shard, (1 - group) * half, half, cut_axis)
-    firsts = over_fs(mine, fs)
+    firsts = over_fs(mine, fs, relay)
     seconds = [other] + [
         lax.ppermute(firsts[mask], "grp", [(0, 1), (1, 0)]) for mask in range(1, fs)
     ]
@@ -135,8 +135,8 @@
         scales = jnp.stack([scale_out, scale_down])
         all_scales = [scales] + [swap(scales, "fs", fs, mask) for mask in range(1, fs)]
         out_mine, out_other = gather_weight(weight_out.astype(jnp.bfloat16), 0, fs)
-        up_mine, up_other = gather_weight(weight_up.astype(jnp.bfloat16), 1, fs)
-        down_mine, down_other = gather_weight(weight_down.astype(jnp.bfloat16), 0, fs)
+        up_mine, up_other = gather_weight(weight_up.astype(jnp.bfloat16), 1, fs, relay=True)
+        down_mine, down_other = gather_weight(weight_down.astype(jnp.bfloat16), 0, fs, relay=True)
 
         normed_in = normed_blocks(token_blocks, norm1_gain, fs, tp)
         full_u = jnp.concatenate(

time: 439 us -> 425 us (0.968); the launches traced: 438 us -> 419 us
  matrix products: 60.2 us -> 43 us
  waiting for transfers between devices: 233 us -> 223 us
  other arithmetic: 28.2 us -> 33.1 us
  local copies, waits for them, and re-layouts: 19.3 us -> 23.9 us
    dot_general x1, matrix products: 32.6 us -> 14.9 us  [layer(): pre_up = jnp.dot(normed_mid, full_up, preferred_element_type=jnp.float32)]
    ppermute x4 -> x2, waiting for transfers between devices: 4.91 us -> 0.01 us  [over_fs(): relayed = lax.ppermute(far, 'fs', [(1, 0), (2, 3)])]
    ppermute x23 -> x25, waiting for transfers between devices: 154 us -> 152 us  [swap(): return lax.ppermute(value, axis, [(k, k ^ mask) for k in range(size)])]
    ppermute x23 -> x25, starting transfers between devices: 67.4 us -> 69.2 us  [swap(): return lax.ppermute(value, axis, [(k, k ^ mask) for k in range(size)])]
  transfers between devices with their start and end apart: 43 -> 41, of which waited for: 17 -> 16; matrix products, arithmetic and copies ran while one was open for 21% -> 21% of each run, Pallas kernels for 0% -> 0%
where the time goes in v2:
time: 425 us; the launch traced here: 419 us
  waiting for transfers between devices  223 us (52%)
  starting transfers between devices  88.4 us (21%)
  matrix products  43 us (10%)
  other arithmetic  33.1 us (8%)
  local copies, waits for them, and re-layouts  23.9 us (6%)
  blocking collectives  6.51 us (2%)
    ppermute x25, waiting for transfers between devices, swap(): return lax.ppermute(value, axis, [(k, k ^ mask) for k in range(size)])  152 us
    ppermute x12, waiting for transfers between devices, gather_weight(): lax.ppermute(firsts[mask], 'grp', [(0, 1), (1, 0)])  71.2 us
    ppermute x25, starting transfers between devices, swap(): return lax.ppermute(value, axis, [(k, k ^ mask) for k in range(size)])  69.2 us
    dot_general x4, matrix products, layer(): jnp.dot(hidden, jnp.concatenate([a, b]), preferred_element_type=jnp.float32)  17 us
    dot_general x1, matrix products, layer(): pre_up = jnp.dot(normed_mid, full_up, preferred_element_type=jnp.float32)  14.9 us
    ppermute x12, starting transfers between devices, gather_weight(): lax.ppermute(firsts[mask], 'grp', [(0, 1), (1, 0)])  14.3 us
  transfers between devices with their start and end apart: 41, of which 16 were waited for; matrix products, arithmetic and copies ran while one was open for 21% of the time, Pallas kernels for 0%

profile of v2, /device:TPU:0, one launch (start us, length us, event | category | flops | bytes accessed | tf_op | source)
XLA Modules:
  0.0 418.8 jit_solution(9864615824853017919)
XLA Ops:
  0.0 3.0 collective-permute-start.1
  6.0 1.6 collective-permute-start.3
  7.6 2.6 collective-permute-start.5
  12.0 1.8 slice_bitcast_fusion.14
  20.4 2.8 collective-permute-start.14
  25.1 2.5 collective-permute-start.17
  28.2 2.6 collective-permute-done.17
  30.9 2.5 collective-permute-start.7
  33.9 1.6 slice_bitcast_fusion.13
  35.6 1.5 collective-permute-start.4
  37.1 1.6 slice_bitcast_fusion.11
  42.1 2.8 collective-permute-done.4
  47.2 1.6 collective-permute-start.12
  49.6 2.2 collective-permute-start.15
  52.5 7.5 %collective-permute-done.12 = bf16[128,512]{1,0:T(8,128)(2,1)S(1)} collective-permute-done((bf16[128,512]{1,0:T(8,128)(2,1)S(1)}, bf16[128,512]{1,0:T(8,128)(2,1)S(1)}, u32[]{:S(2)}, u32[]{:S(2)}) %collective-permute-start.12) | collective-permute-done | bytes 131104 | tf_op jit(solution)/shard_map/ppermute | solution.py:12
  60.6 1.5 collective-permute-start.13
  65.4 1.6 pad_maximum_fusion
  68.1 2.4 fusion.170
  70.6 6.5 %all-reduce = (f32[1024]{0:T(1024)S(1)}, f32[1024]{0:T(1024)S(1)}) all-reduce(f32[1024]{0:T(1024)S(1)} %get-tuple-element.6, f32[1024]{0:T(1024)S(1)} %get-tuple-element.5), channel_id=1, replica_groups=mesh['grp'=2,'fs'=4,'tp'=4] {'tp'}, use_global_device_ids=true, to_apply=%region_7.8 | all-reduce | flops 2048 | bytes 16384 | tf_op jit(solution)/shard_map/psum | solution.py:153
  77.1 1.7 multiply_convert_fusion.9
  80.1 2.7 fusion.99
  88.3 1.7 dynamic-slice_bitcast_fusion.3
  91.0 2.5 convert_element_type.251
  93.5 1.6 constant_dynamic-slice_fusion.2
  95.2 2.7 collective-permute-start.26
  98.1 2.9 fusion.57
  101.7 2.5 convert_element_type.253
  106.0 1.6 collective-permute-start.28
  107.6 59.7 %collective-permute-done.26 = bf16[512,1024]{1,0:T(8,128)(2,1)} collective-permute-done((bf16[512,1024]{1,0:T(8,128)(2,1)}, bf16[512,1024]{1,0:T(8,128)(2,1)}, u32[]{:S(2)}, u32[]{:S(2)}) %collective-permute-start.26) | collective-permute-done | bytes 1048608 | tf_op jit(solution)/shard_map/ppermute | solution.py:12
  169.4 2.8 fusion.29
  172.7 17.1 %collective-permute-done.33 = bf16[1024,512]{1,0:T(8,128)(2,1)} collective-permute-done((bf16[1024,512]{1,0:T(8,128)(2,1)}, bf16[1024,512]{1,0:T(8,128)(2,1)}, u32[]{:S(2)}, u32[]{:S(2)}) %collective-permute-start.33) | collective-permute-done | bytes 1048608 | tf_op jit(solution)/shard_map/ppermute | solution.py:12
  191.2 21.7 %collective-permute-start.24 = (bf16[512,1024]{1,0:T(8,128)(2,1)}, bf16[512,1024]{1,0:T(8,128)(2,1)}, u32[]{:S(2)}, u32[]{:S(2)}) collective-permute-start(bf16[512,1024]{1,0:T(8,128)(2,1)} %get-tuple-element.26), channel_id=1, source_target_pairs={{0,4},{4,0},{8,12},{12,8},{1,5},{5,1},{9,13},{13,9},{2,6},{6,2},{1... | collective-permute-start | bytes 3145736 | tf_op jit(solution)/shard_map/ppermute | solution.py:12
  212.9 22.0 %collective-permute-start.31 = (bf16[1024,512]{1,0:T(8,128)(2,1)}, bf16[1024,512]{1,0:T(8,128)(2,1)}, u32[]{:S(2)}, u32[]{:S(2)}) collective-permute-start(bf16[1024,512]{1,0:T(8,128)(2,1)} %get-tuple-element.24), channel_id=1, source_target_pairs={{0,4},{4,0},{8,12},{12,8},{1,5},{5,1},{9,13},{13,9},{2,6},{6,2},{1... | collective-permute-start | bytes 3145736 | tf_op jit(solution)/shard_map/ppermute | solution.py:12
  237.9 1.5 collective-permute-start.27
  239.4 2.3 broadcast_select_fusion
  242.0 14.9 %collective-permute-done.24 = bf16[512,1024]{1,0:T(8,128)(2,1)} collective-permute-done((bf16[512,1024]{1,0:T(8,128)(2,1)}, bf16[512,1024]{1,0:T(8,128)(2,1)}, u32[]{:S(2)}, u32[]{:S(2)}) %collective-permute-start.24) | collective-permute-done | bytes 1048608 | tf_op jit(solution)/shard_map/ppermute | solution.py:12
  258.4 20.9 %collective-permute-done.31 = bf16[1024,512]{1,0:T(8,128)(2,1)} collective-permute-done((bf16[1024,512]{1,0:T(8,128)(2,1)}, bf16[1024,512]{1,0:T(8,128)(2,1)}, u32[]{:S(2)}, u32[]{:S(2)}) %collective-permute-start.31) | collective-permute-done | bytes 1048608 | tf_op jit(solution)/shard_map/ppermute | solution.py:12
  281.6 1.5 collective-permute-start.30
  284.0 2.0 fusion.56
  286.7 22.5 %collective-permute-done.25 = bf16[512,1024]{1,0:T(8,128)(2,1)S(1)} collective-permute-done((bf16[512,1024]{1,0:T(8,128)(2,1)}, bf16[512,1024]{1,0:T(8,128)(2,1)S(1)}, u32[]{:S(2)}, u32[]{:S(2)}) %collective-permute-start.25) | collective-permute-done | bytes 1048608 | tf_op jit(solution)/shard_map/ppermute | solution.py:34
  309.1 44.9 %collective-permute-done.30 = bf16[512,1024]{1,0:T(8,128)(2,1)S(1)} collective-permute-done((bf16[512,1024]{1,0:T(8,128)(2,1)S(1)}, bf16[512,1024]{1,0:T(8,128)(2,1)S(1)}, u32[]{:S(2)}, u32[]{:S(2)}) %collective-permute-start.30) | collective-permute-done | bytes 1048608 | tf_op jit(solution)/shard_map/ppermute | solution.py:34
  355.1 14.9 %multiply_convert_fusion = bf16[1024,2048]{1,0:T(8,128)(2,1)} fusion(f32[2048]{0:T(1024)S(1)} %pad_maximum_fusion.7, bf16[512,1024]{1,0:T(8,128)(2,1)} %copy-done.38, bf16[512,1024]{1,0:T(8,128)(2,1)} %copy-done.14, bf16[512,1024]{1,0:T(8,128)(2,1)} %copy-done.36, bf16[512,1024]{1,0:T(8,128)(2,1)} %collective-permute-done.26, ...), kind=kOutput, calls=%fused_computation.16 | convolution fusion | flops 8682209280 | bytes 16785408 | tf_op jit(solution)/shard_map/dot_general | solution.py:185
  370.0 5.0 %fusion.79 = bf16[1,1024,512]{1,2,0:T(8,128)(2,1)S(1)} fusion(bf16[1024,2048]{1,0:T(8,128)(2,1)} %multiply_convert_fusion, bf16[1024,512]{1,0:T(8,128)(2,1)S(1)} %copy-done.5, bf16[1024,512]{1,0:T(8,128)(2,1)} %get-tuple-element.24, f32[512]{0:T(512)S(1)} %copy-done.30), kind=kOutput, calls=%fused_computation.105 | convolution fusion | flops 2152726528 | bytes 7342080 | tf_op jit(solution)/shard_map/dot_general | solution.py:189
  375.1 4.2 fusion.82
  379.2 3.9 fusion.85
  383.2 3.9 fusion.88
  388.5 2.1 collective-permute-done.39
  392.1 24.2 %collective-permute-done.40 = bf16[1024,512]{0,1:T(8,128)(2,1)S(1)} collective-permute-done((bf16[1024,512]{0,1:T(8,128)(2,1)S(1)}, bf16[1024,512]{0,1:T(8,128)(2,1)S(1)}, u32[]{:S(2)}, u32[]{:S(2)}) %collective-permute-start.40) | collective-permute-done | bytes 1048608 | tf_op jit(solution)/shard_map/ppermute | solution.py:12
  (184 shorter events, 55.2 us)
Async XLA Ops:
  0.0 46.5 %collective-permute-start.1 = (bf16[1024,512]{1,0:T(8,128)(2,1)}, bf16[1024,512]{1,0:T(8,128)(2,1)S(1)}, u32[]{:S(2)}, u32[]{:S(2)}) collective-permute-start(bf16[1024,512]{1,0:T(8,128)(2,1)} %param.16), channel_id=1, source_target_pairs={{0,2},{1,3},{2,0},{3,1},{4,6},{5,7},{6,4},{7,5},{8,10},{9,11},{10,... | collective-permute-start | bytes 3145736 | tf_op jit(solution)/shard_map/ppermute | solution.py:12
  3.1 60.5 %collective-permute-start = (bf16[1024,512]{1,0:T(8,128)(2,1)}, bf16[1024,512]{1,0:T(8,128)(2,1)}, u32[]{:S(2)}, u32[]{:S(2)}) collective-permute-start(bf16[1024,512]{1,0:T(8,128)(2,1)} %param.16), channel_id=1, source_target_pairs={{0,1},{1,0},{2,3},{3,2},{4,5},{5,4},{6,7},{7,6},{8,9},{9,8},{10,11... | collective-permute-start | bytes 3145736 | tf_op jit(solution)/shard_map/ppermute | solution.py:12
  6.0 27.9 %collective-permute-start.3 = (bf16[512,2,128]{2,0,1:T(8,128)(2,1)S(1)}, bf16[512,2,128]{2,0,1:T(8,128)(2,1)}, u32[]{:S(2)}, u32[]{:S(2)}) collective-permute-start(bf16[512,2,128]{2,0,1:T(8,128)(2,1)S(1)} %get-tuple-element.28), channel_id=1, source_target_pairs={{0,4},{4,0},{8,12},{12,8},{1,5},{5,1},{9,13},{13,9},{2,6},{6,2},{1... | collective-permute-start | bytes 786440 | tf_op jit(solution)/shard_map/ppermute | solution.py:12
  7.6 28.0 %collective-permute-start.5 = (bf16[512,2,128]{2,0,1:T(8,128)(2,1)S(1)}, bf16[512,2,128]{2,0,1:T(8,128)(2,1)}, u32[]{:S(2)}, u32[]{:S(2)}) collective-permute-start(bf16[512,2,128]{2,0,1:T(8,128)(2,1)S(1)} %get-tuple-element.28), channel_id=1, source_target_pairs={{0,8},{4,12},{8,0},{12,4},{1,9},{5,13},{9,1},{13,5},{2,10},{6,14},... | collective-permute-start | bytes 786440 | tf_op jit(solution)/shard_map/ppermute | solution.py:12
  10.8 9.6 %collective-permute-start.11 = (f32[2,512]{1,0:T(2,128)}, f32[2,512]{1,0:T(2,128)}, u32[]{:S(2)}, u32[]{:S(2)}) collective-permute-start(f32[2,512]{1,0:T(2,128)} %pad_maximum_fusion.8), channel_id=1, source_target_pairs={{0,4},{4,0},{8,12},{12,8},{1,5},{5,1},{9,13},{13,9},{2,6},{6,2},{1... | collective-permute-start | bytes 12296 | tf_op jit(solution)/shard_map/ppermute | solution.py:12
  20.1 27.1 %copy-start.16 = (bf16[128,512]{1,0:T(8,128)(2,1)S(1)}, bf16[128,512]{1,0:T(8,128)(2,1)}, u32[]{:S(2)}) copy-start(bf16[128,512]{1,0:T(8,128)(2,1)} %get-tuple-element.30) | copy-start | bytes 393220
  20.4 4.7 %collective-permute-start.14 = (f32[2,512]{1,0:T(2,128)}, f32[2,512]{1,0:T(2,128)S(1)}, u32[]{:S(2)}, u32[]{:S(2)}) collective-permute-start(f32[2,512]{1,0:T(2,128)} %pad_maximum_fusion.8), channel_id=1, source_target_pairs={{0,8},{4,12},{8,0},{12,4},{1,9},{5,13},{9,1},{13,5},{2,10},{6,14},... | collective-permute-start | bytes 12296 | tf_op jit(solution)/shard_map/ppermute | solution.py:12
  25.1 5.7 %collective-permute-start.17 = (f32[2,512]{1,0:T(2,128)}, f32[2,512]{1,0:T(2,128)S(1)}, u32[]{:S(2)}, u32[]{:S(2)}) collective-permute-start(f32[2,512]{1,0:T(2,128)} %pad_maximum_fusion.8), channel_id=1, source_target_pairs={{0,12},{4,8},{8,4},{12,0},{1,13},{5,9},{9,5},{13,1},{2,14},{6,10},... | collective-permute-start | bytes 12296 | tf_op jit(solution)/shard_map/ppermute | solution.py:12
  30.9 9.1 %collective-permute-start.7 = (bf16[512,2,128]{2,0,1:T(8,128)(2,1)S(1)}, bf16[512,2,128]{2,0,1:T(8,128)(2,1)S(1)}, u32[]{:S(2)}, u32[]{:S(2)}) collective-permute-start(bf16[512,2,128]{2,0,1:T(8,128)(2,1)S(1)} %get-tuple-element.28), channel_id=1, source_target_pairs={{0,12},{4,8},{8,4},{12,0},{1,13},{5,9},{9,5},{13,1},{2,14},{6,10},... | collective-permute-start | bytes 786440 | tf_op jit(solution)/shard_map/ppermute | solution.py:12
  33.9 13.2 %collective-permute-start.9 = (bf16[128,512]{1,0:T(8,128)(2,1)}, bf16[128,512]{1,0:T(8,128)(2,1)}, u32[]{:S(2)}, u32[]{:S(2)}) collective-permute-start(bf16[128,512]{1,0:T(8,128)(2,1)} %get-tuple-element.30), channel_id=1, source_target_pairs={{0,4},{4,0},{8,12},{12,8},{1,5},{5,1},{9,13},{13,9},{2,6},{6,2},{1... | collective-permute-start | bytes 393224 | tf_op jit(solution)/shard_map/ppermute | solution.py:12
  35.6 9.4 %collective-permute-start.4 = (bf16[512,2,128]{2,0,1:T(8,128)(2,1)}, bf16[512,2,128]{2,0,1:T(8,128)(2,1)S(1)}, u32[]{:S(2)}, u32[]{:S(2)}) collective-permute-start(bf16[512,2,128]{2,0,1:T(8,128)(2,1)} %collective-permute-done.3), channel_id=1, source_target_pairs={{0,16},{16,0},{1,17},{17,1},{2,18},{18,2},{3,19},{19,3},{4,20},{20... | collective-permute-start | bytes 786440 | tf_op jit(solution)/shard_map/ppermute | solution.py:34
  39.9 9.7 %collective-permute-start.6 = (bf16[512,2,128]{2,0,1:T(8,128)(2,1)}, bf16[512,2,128]{2,0,1:T(8,128)(2,1)S(1)}, u32[]{:S(2)}, u32[]{:S(2)}) collective-permute-start(bf16[512,2,128]{2,0,1:T(8,128)(2,1)} %collective-permute-done.5), channel_id=1, source_target_pairs={{0,16},{16,0},{1,17},{17,1},{2,18},{18,2},{3,19},{19,3},{4,20},{20... | collective-permute-start | bytes 786440 | tf_op jit(solution)/shard_map/ppermute | solution.py:34
  45.0 17.1 %collective-permute-start.8 = (bf16[512,2,128]{2,0,1:T(8,128)(2,1)S(1)}, bf16[512,2,128]{2,0,1:T(8,128)(2,1)S(1)}, u32[]{:S(2)}, u32[]{:S(2)}) collective-permute-start(bf16[512,2,128]{2,0,1:T(8,128)(2,1)S(1)} %collective-permute-done.7), channel_id=1, source_target_pairs={{0,16},{16,0},{1,17},{17,1},{2,18},{18,2},{3,19},{19,3},{4,20},{20... | collective-permute-start | bytes 786440 | tf_op jit(solution)/shard_map/ppermute | solution.py:34
  46.5 18.6 %collective-permute-start.2 = (bf16[1024,512]{1,0:T(8,128)(2,1)S(1)}, bf16[1024,512]{1,0:T(8,128)(2,1)S(1)}, u32[]{:S(2)}, u32[]{:S(2)}) collective-permute-start(bf16[1024,512]{1,0:T(8,128)(2,1)S(1)} %collective-permute-done.1), channel_id=1, source_target_pairs={{0,1},{1,0},{2,3},{3,2},{4,5},{5,4},{6,7},{7,6},{8,9},{9,8},{10,11... | collective-permute-start | bytes 3145736 | tf_op jit(solution)/shard_map/ppermute | solution.py:12
  47.2 12.9 %collective-permute-start.12 = (bf16[128,512]{1,0:T(8,128)(2,1)S(1)}, bf16[128,512]{1,0:T(8,128)(2,1)S(1)}, u32[]{:S(2)}, u32[]{:S(2)}) collective-permute-start(bf16[128,512]{1,0:T(8,128)(2,1)S(1)} %copy-done.16), channel_id=1, source_target_pairs={{0,8},{4,12},{8,0},{12,4},{1,9},{5,13},{9,1},{13,5},{2,10},{6,14},... | collective-permute-start | bytes 393224 | tf_op jit(solution)/shard_map/ppermute | solution.py:12
  49.6 10.9 %collective-permute-start.15 = (bf16[128,512]{1,0:T(8,128)(2,1)S(1)}, bf16[128,512]{1,0:T(8,128)(2,1)S(1)}, u32[]{:S(2)}, u32[]{:S(2)}) collective-permute-start(bf16[128,512]{1,0:T(8,128)(2,1)S(1)} %copy-done.16), channel_id=1, source_target_pairs={{0,12},{4,8},{8,4},{12,0},{1,13},{5,9},{9,5},{13,1},{2,14},{6,10},... | collective-permute-start | bytes 393224 | tf_op jit(solution)/shard_map/ppermute | solution.py:12
  60.0 23.3 %collective-permute-start.10 = (bf16[128,512]{1,0:T(8,128)(2,1)}, bf16[128,512]{1,0:T(8,128)(2,1)}, u32[]{:S(2)}, u32[]{:S(2)}) collective-permute-start(bf16[128,512]{1,0:T(8,128)(2,1)} %collective-permute-done.9), channel_id=1, source_target_pairs={{0,16},{16,0},{1,17},{17,1},{2,18},{18,2},{3,19},{19,3},{4,20},{20... | collective-permute-start | bytes 393224 | tf_op jit(solution)/shard_map/ppermute | solution.py:34
  60.6 24.3 %collective-permute-start.13 = (bf16[128,512]{1,0:T(8,128)(2,1)S(1)}, bf16[128,512]{1,0:T(8,128)(2,1)}, u32[]{:S(2)}, u32[]{:S(2)}) collective-permute-start(bf16[128,512]{1,0:T(8,128)(2,1)S(1)} %collective-permute-done.12), channel_id=1, source_target_pairs={{0,16},{16,0},{1,17},{17,1},{2,18},{18,2},{3,19},{19,3},{4,20},{20... | collective-permute-start | bytes 393224 | tf_op jit(solution)/shard_map/ppermute | solution.py:34
  62.1 24.2 %collective-permute-start.16 = (bf16[128,512]{1,0:T(8,128)(2,1)S(1)}, bf16[128,512]{1,0:T(8,128)(2,1)}, u32[]{:S(2)}, u32[]{:S(2)}) collective-permute-start(bf16[128,512]{1,0:T(8,128)(2,1)S(1)} %collective-permute-done.15), channel_id=1, source_target_pairs={{0,16},{16,0},{1,17},{17,1},{2,18},{18,2},{3,19},{19,3},{4,20},{20... | collective-permute-start | bytes 393224 | tf_op jit(solution)/shard_map/ppermute | solution.py:34
  91.0 7.1 %collective-permute-start.19 = (bf16[1024,512]{0,1:T(8,128)(2,1)}, bf16[1024,512]{0,1:T(8,128)(2,1)}, u32[]{:S(2)}, u32[]{:S(2)}) collective-permute-start(bf16[1024,512]{0,1:T(8,128)(2,1)} %get-tuple-element.22), channel_id=1, source_target_pairs={{0,1},{1,0},{2,3},{3,2},{4,5},{5,4},{6,7},{7,6},{8,9},{9,8},{10,11... | collective-permute-start | bytes 3145736 | tf_op jit(solution)/shard_map/ppermute | solution.py:12
  95.2 72.2 %collective-permute-start.26 = (bf16[512,1024]{1,0:T(8,128)(2,1)}, bf16[512,1024]{1,0:T(8,128)(2,1)}, u32[]{:S(2)}, u32[]{:S(2)}) collective-permute-start(bf16[512,1024]{1,0:T(8,128)(2,1)} %get-tuple-element.26), channel_id=1, source_target_pairs={{0,8},{4,12},{8,0},{12,4},{1,9},{5,13},{9,1},{13,5},{2,10},{6,14},... | collective-permute-start | bytes 3145736 | tf_op jit(solution)/shard_map/ppermute | solution.py:12
  97.9 70.2 %collective-permute-start.18 = (bf16[1024,512]{0,1:T(8,128)(2,1)}, bf16[1024,512]{0,1:T(8,128)(2,1)}, u32[]{:S(2)}, u32[]{:S(2)}) collective-permute-start(bf16[1024,512]{0,1:T(8,128)(2,1)} %get-tuple-element.21), channel_id=1, source_target_pairs={{0,1},{1,0},{2,3},{3,2},{4,5},{5,4},{6,7},{7,6},{8,9},{9,8},{10,11... | collective-permute-start | bytes 3145736 | tf_op jit(solution)/shard_map/ppermute | solution.py:12
  101.0 68.4 %collective-permute-start.20 = (bf16[1024,512]{0,1:T(8,128)(2,1)}, bf16[1024,512]{0,1:T(8,128)(2,1)}, u32[]{:S(2)}, u32[]{:S(2)}) collective-permute-start(bf16[1024,512]{0,1:T(8,128)(2,1)} %fusion.57), channel_id=1, source_target_pairs={{0,2},{1,3},{2,0},{3,1},{4,6},{5,7},{6,4},{7,5},{8,10},{9,11},{10,... | collective-permute-start | bytes 3145736 | tf_op jit(solution)/shard_map/ppermute | solution.py:12
  105.7 84.2 %collective-permute-start.33 = (bf16[1024,512]{1,0:T(8,128)(2,1)}, bf16[1024,512]{1,0:T(8,128)(2,1)}, u32[]{:S(2)}, u32[]{:S(2)}) collective-permute-start(bf16[1024,512]{1,0:T(8,128)(2,1)} %get-tuple-element.24), channel_id=1, source_target_pairs={{0,8},{4,12},{8,0},{12,4},{1,9},{5,13},{9,1},{13,5},{2,10},{6,14},... | collective-permute-start | bytes 3145736 | tf_op jit(solution)/shard_map/ppermute | solution.py:12
  106.0 85.2 %collective-permute-start.28 = (bf16[512,1024]{1,0:T(8,128)(2,1)}, bf16[512,1024]{1,0:T(8,128)(2,1)}, u32[]{:S(2)}, u32[]{:S(2)}) collective-permute-start(bf16[512,1024]{1,0:T(8,128)(2,1)} %get-tuple-element.26), channel_id=1, source_target_pairs={{4,8},{8,4},{5,9},{9,5},{6,10},{10,6},{7,11},{11,7},{20,24},{24,20... | collective-permute-start | bytes 3145736 | tf_op jit(solution)/shard_map/ppermute | solution.py:20
  107.6 128.2 %copy-start.22 = (f32[2048]{0:T(1024)S(1)}, f32[2048]{0:T(1024)}, u32[]{:S(2)}) copy-start(f32[2048]{0:T(1024)} %param.27) | copy-start | bytes 24580
  107.6 128.3 %copy-start.23 = (f32[2048]{0:T(1024)S(1)}, f32[2048]{0:T(1024)}, u32[]{:S(2)}) copy-start(f32[2048]{0:T(1024)} %param.29) | copy-start | bytes 24580
  167.3 45.6 %collective-permute-start.35 = (bf16[1024,512]{1,0:T(8,128)(2,1)}, bf16[1024,512]{1,0:T(8,128)(2,1)S(1)}, u32[]{:S(2)}, u32[]{:S(2)}) collective-permute-start(bf16[1024,512]{1,0:T(8,128)(2,1)} %get-tuple-element.24), channel_id=1, source_target_pairs={{4,8},{8,4},{5,9},{9,5},{6,10},{10,6},{7,11},{11,7},{20,24},{24,20... | collective-permute-start | bytes 3145736 | tf_op jit(solution)/shard_map/ppermute | solution.py:20
  168.1 66.8 %collective-permute-start.29 = (bf16[512,1024]{1,0:T(8,128)(2,1)}, bf16[512,1024]{1,0:T(8,128)(2,1)S(1)}, u32[]{:S(2)}, u32[]{:S(2)}) collective-permute-start(bf16[512,1024]{1,0:T(8,128)(2,1)} %collective-permute-done.26), channel_id=1, source_target_pairs={{4,0},{8,12},{5,1},{9,13},{6,2},{10,14},{7,3},{11,15},{20,16},{24,... | collective-permute-start | bytes 3145736 | tf_op jit(solution)/shard_map/ppermute | solution.py:21
  172.2 63.7 %collective-permute-start.22 = (bf16[1024,512]{0,1:T(8,128)(2,1)S(1)}, bf16[1024,512]{0,1:T(8,128)(2,1)S(1)}, u32[]{:S(2)}, u32[]{:S(2)}) collective-permute-start(bf16[1024,512]{0,1:T(8,128)(2,1)S(1)} %get-tuple-element.10), channel_id=1, source_target_pairs={{0,2},{1,3},{2,0},{3,1},{4,6},{5,7},{6,4},{7,5},{8,10},{9,11},{10,... | collective-permute-start | bytes 3145736 | tf_op jit(solution)/shard_map/ppermute | solution.py:12
  189.9 48.0 %collective-permute-start.36 = (bf16[1024,512]{1,0:T(8,128)(2,1)}, bf16[1024,512]{1,0:T(8,128)(2,1)}, u32[]{:S(2)}, u32[]{:S(2)}) collective-permute-start(bf16[1024,512]{1,0:T(8,128)(2,1)} %collective-permute-done.33), channel_id=1, source_target_pairs={{4,0},{8,12},{5,1},{9,13},{6,2},{10,14},{7,3},{11,15},{20,16},{24,... | collective-permute-start | bytes 3145736 | tf_op jit(solution)/shard_map/ppermute | solution.py:21
  191.2 65.8 %collective-permute-start.24 = (bf16[512,1024]{1,0:T(8,128)(2,1)}, bf16[512,1024]{1,0:T(8,128)(2,1)}, u32[]{:S(2)}, u32[]{:S(2)}) collective-permute-start(bf16[512,1024]{1,0:T(8,128)(2,1)} %get-tuple-element.26), channel_id=1, source_target_pairs={{0,4},{4,0},{8,12},{12,8},{1,5},{5,1},{9,13},{13,9},{2,6},{6,2},{1... | collective-permute-start | bytes 3145736 | tf_op jit(solution)/shard_map/ppermute | solution.py:12
  212.9 66.4 %collective-permute-start.31 = (bf16[1024,512]{1,0:T(8,128)(2,1)}, bf16[1024,512]{1,0:T(8,128)(2,1)}, u32[]{:S(2)}, u32[]{:S(2)}) collective-permute-start(bf16[1024,512]{1,0:T(8,128)(2,1)} %get-tuple-element.24), channel_id=1, source_target_pairs={{0,4},{4,0},{8,12},{12,8},{1,5},{5,1},{9,13},{13,9},{2,6},{6,2},{1... | collective-permute-start | bytes 3145736 | tf_op jit(solution)/shard_map/ppermute | solution.py:12
  235.8 44.9 %collective-permute-start.21 = (bf16[1024,512]{0,1:T(8,128)(2,1)S(1)}, bf16[1024,512]{0,1:T(8,128)(2,1)S(1)}, u32[]{:S(2)}, u32[]{:S(2)}) collective-permute-start(bf16[1024,512]{0,1:T(8,128)(2,1)S(1)} %get-tuple-element.10), channel_id=1, source_target_pairs={{0,1},{1,0},{2,3},{3,2},{4,5},{5,4},{6,7},{7,6},{8,9},{9,8},{10,11... | collective-permute-start | bytes 3145736 | tf_op jit(solution)/shard_map/ppermute | solution.py:12
  235.9 45.6 %collective-permute-start.23 = (bf16[1024,512]{0,1:T(8,128)(2,1)S(1)}, bf16[1024,512]{0,1:T(8,128)(2,1)S(1)}, u32[]{:S(2)}, u32[]{:S(2)}) collective-permute-start(bf16[1024,512]{0,1:T(8,128)(2,1)S(1)} %collective-permute-done.22), channel_id=1, source_target_pairs={{0,1},{1,0},{2,3},{3,2},{4,5},{5,4},{6,7},{7,6},{8,9},{9,8},{10,11... | collective-permute-start | bytes 3145736 | tf_op jit(solution)/shard_map/ppermute | solution.py:12
  237.9 43.7 %copy-start.14 = (bf16[512,1024]{1,0:T(8,128)(2,1)}, bf16[512,1024]{1,0:T(8,128)(2,1)S(1)}, u32[]{:S(2)}) copy-start(bf16[512,1024]{1,0:T(8,128)(2,1)S(1)} %broadcast_select_fusion.1) | copy-start | bytes 3145732
  237.9 48.1 %collective-permute-start.27 = (bf16[512,1024]{1,0:T(8,128)(2,1)}, bf16[512,1024]{1,0:T(8,128)(2,1)S(1)}, u32[]{:S(2)}, u32[]{:S(2)}) collective-permute-start(bf16[512,1024]{1,0:T(8,128)(2,1)} %collective-permute-done.26), channel_id=1, source_target_pairs={{0,16},{16,0},{1,17},{17,1},{2,18},{18,2},{3,19},{19,3},{4,20},{20... | collective-permute-start | bytes 3145736 | tf_op jit(solution)/shard_map/ppermute | solution.py:34
  256.9 122.3 %collective-permute-start.34 = (bf16[1024,512]{1,0:T(8,128)(2,1)}, bf16[1024,512]{1,0:T(8,128)(2,1)}, u32[]{:S(2)}, u32[]{:S(2)}) collective-permute-start(bf16[1024,512]{1,0:T(8,128)(2,1)} %collective-permute-done.33), channel_id=1, source_target_pairs={{0,16},{16,0},{1,17},{17,1},{2,18},{18,2},{3,19},{19,3},{4,20},{20... | collective-permute-start | bytes 3145736 | tf_op jit(solution)/shard_map/ppermute | solution.py:34
  279.3 29.8 %collective-permute-start.25 = (bf16[512,1024]{1,0:T(8,128)(2,1)}, bf16[512,1024]{1,0:T(8,128)(2,1)S(1)}, u32[]{:S(2)}, u32[]{:S(2)}) collective-permute-start(bf16[512,1024]{1,0:T(8,128)(2,1)} %collective-permute-done.24), channel_id=1, source_target_pairs={{0,16},{16,0},{1,17},{17,1},{2,18},{18,2},{3,19},{19,3},{4,20},{20... | collective-permute-start | bytes 3145736 | tf_op jit(solution)/shard_map/ppermute | solution.py:34
  280.8 94.2 %collective-permute-start.32 = (bf16[1024,512]{1,0:T(8,128)(2,1)}, bf16[1024,512]{1,0:T(8,128)(2,1)}, u32[]{:S(2)}, u32[]{:S(2)}) collective-permute-start(bf16[1024,512]{1,0:T(8,128)(2,1)} %collective-permute-done.31), channel_id=1, source_target_pairs={{0,16},{16,0},{1,17},{17,1},{2,18},{18,2},{3,19},{19,3},{4,20},{20... | collective-permute-start | bytes 3145736 | tf_op jit(solution)/shard_map/ppermute | solution.py:34
  281.6 72.5 %collective-permute-start.30 = (bf16[512,1024]{1,0:T(8,128)(2,1)S(1)}, bf16[512,1024]{1,0:T(8,128)(2,1)S(1)}, u32[]{:S(2)}, u32[]{:S(2)}) collective-permute-start(bf16[512,1024]{1,0:T(8,128)(2,1)S(1)} %broadcast_select_fusion.1), channel_id=1, source_target_pairs={{0,16},{16,0},{1,17},{17,1},{2,18},{18,2},{3,19},{19,3},{4,20},{20... | collective-permute-start | bytes 3145736 | tf_op jit(solution)/shard_map/ppermute | solution.py:34
  284.0 71.1 %copy-start.4 = (bf16[512,1024]{1,0:T(8,128)(2,1)S(1)}, bf16[512,1024]{1,0:T(8,128)(2,1)}, u32[]{:S(2)}) copy-start(bf16[512,1024]{1,0:T(8,128)(2,1)} %get-tuple-element.25) | copy-start | bytes 3145732
  286.0 68.0 %copy-start.36 = (bf16[512,1024]{1,0:T(8,128)(2,1)}, bf16[512,1024]{1,0:T(8,128)(2,1)S(1)}, u32[]{:S(2)}) copy-start(bf16[512,1024]{1,0:T(8,128)(2,1)S(1)} %collective-permute-done.27) | copy-start | bytes 3145732
  286.0 97.1 %collective-permute-start.37 = (bf16[1024,512]{1,0:T(8,128)(2,1)}, bf16[1024,512]{1,0:T(8,128)(2,1)}, u32[]{:S(2)}, u32[]{:S(2)}) collective-permute-start(bf16[1024,512]{1,0:T(8,128)(2,1)} %broadcast_select_fusion), channel_id=1, source_target_pairs={{0,16},{16,0},{1,17},{17,1},{2,18},{18,2},{3,19},{19,3},{4,20},{20... | collective-permute-start | bytes 3145736 | tf_op jit(solution)/shard_map/ppermute | solution.py:34
  309.1 44.9 %copy-start.37 = (bf16[512,1024]{1,0:T(8,128)(2,1)}, bf16[512,1024]{1,0:T(8,128)(2,1)S(1)}, u32[]{:S(2)}) copy-start(bf16[512,1024]{1,0:T(8,128)(2,1)S(1)} %collective-permute-done.25) | copy-start | bytes 3145732
  387.9 2.7 collective-permute-start.39
  388.0 4.1 collective-permute-start.38
  391.0 25.3 %collective-permute-start.40 = (bf16[1024,512]{0,1:T(8,128)(2,1)S(1)}, bf16[1024,512]{0,1:T(8,128)(2,1)S(1)}, u32[]{:S(2)}, u32[]{:S(2)}) collective-permute-start(bf16[1024,512]{0,1:T(8,128)(2,1)S(1)} %fusion.47), channel_id=1, source_target_pairs={{0,2},{1,3},{2,0},{3,1},{4,6},{5,7},{6,4},{7,5},{8,10},{9,11},{10,... | collective-permute-start | bytes 3145736 | tf_op jit(solution)/shard_map/ppermute | solution.py:12
  (33 other events, 168.9 us)

commit v3 on v2

--- a/solution.py
+++ b/solution.py
@@ -12,11 +12,11 @@
     return lax.ppermute(value, axis, [(k, k ^ mask) for k in range(size)])
 
 
-def over_fs(piece, fs, relay):
+def over_fs(piece, fs, relay, near_too):
     if fs != 4 or not relay:
         return [piece] + [swap(piece, "fs", fs, mask) for mask in range(1, fs)]
     far = swap(piece, "fs", 4, 2)
-    near = swap(piece, "fs", 4, 1)
+    near = swap(piece, "fs", 4, 1) if near_too else None
     middle = lax.ppermute(piece, "fs", [(1, 2), (2, 1)])
     relayed = lax.ppermute(far, "fs", [(1, 0), (2, 3)])
     me = lax.axis_index("fs")
@@ -24,14 +24,21 @@
     return [piece, near, far, last]
 
 
-def gather_weight(shard, cut_axis, fs, relay=False):
+def gather_weight(shard, cut_axis, fs, relay=False, whole_near=False):
     half = shard.shape[cut_axis] // 2
     group = lax.axis_index("grp")
     mine = lax.dynamic_slice_in_dim(shard, group * half, half, cut_axis)
     other = lax.dynamic_slice_in_dim(shard, (1 - group) * half, half, cut_axis)
-    firsts = over_fs(mine, fs, relay)
+    whole_near = whole_near and relay and fs == 4
+    firsts = over_fs(mine, fs, relay, not whole_near)
+    if whole_near:
+        near = swap(jnp.concatenate([mine, other], axis=cut_axis), "fs", fs, 1)
+        firsts[1], near_other = jnp.split(near, 2, axis=cut_axis)
     seconds = [other] + [
-        lax.ppermute(firsts[mask], "grp", [(0, 1), (1, 0)]) for mask in range(1, fs)
+        near_other
+        if whole_near and mask == 1
+        else lax.ppermute(firsts[mask], "grp", [(0, 1), (1, 0)])
+        for mask in range(1, fs)
     ]
     return firsts, seconds
 
@@ -136,7 +143,7 @@
         all_scales = [scales] + [swap(scales, "fs", fs, mask) for mask in range(1, fs)]
         out_mine, out_other = gather_weight(weight_out.astype(jnp.bfloat16), 0, fs)
         up_mine, up_other = gather_weight(weight_up.astype(jnp.bfloat16), 1, fs, relay=True)
-        down_mine, down_other = gather_weight(weight_down.astype(jnp.bfloat16), 0, fs, relay=True)
+        down_mine, down_other = gather_weight(weight_down.astype(jnp.bfloat16), 0, fs, relay=True, whole_near=True)
 
         normed_in = normed_blocks(token_blocks, norm1_gain, fs, tp)
         full_u = jnp.concatenate(

time: 425 us -> 410 us (0.965); the launches traced: 419 us -> 409 us
  waiting for transfers between devices: 223 us -> 199 us
  matrix products: 43 us -> 60.1 us
  starting transfers between devices: 88.4 us -> 83.2 us
  other arithmetic: 33.1 us -> 37.5 us
    ppermute x25, waiting for transfers between devices: 152 us -> 134 us  [swap(): return lax.ppermute(value, axis, [(k, k ^ mask) for k in range(size)])]
    dot_general x1, matrix products: 14.9 us -> 31.9 us  [layer(): pre_up = jnp.dot(normed_mid, full_up, preferred_element_type=jnp.float32)]
    ppermute x12 -> x11, waiting for transfers between devices: 71.2 us -> 65.1 us  [gather_weight(): lax.ppermute(firsts[mask], 'grp', [(0, 1), (1, 0)])]
    ppermute x25, starting transfers between devices: 69.2 us -> 64.3 us  [swap(): return lax.ppermute(value, axis, [(k, k ^ mask) for k in range(size)])]
    ppermute x12 -> x11, starting transfers between devices: 14.3 us -> 12.8 us  [gather_weight(): lax.ppermute(firsts[mask], 'grp', [(0, 1), (1, 0)])]
  transfers between devices with their start and end apart: 41 -> 40, of which waited for: 16 -> 15; matrix products, arithmetic and copies ran while one was open for 21% -> 26% of each run, Pallas kernels for 0% -> 0%
where the time goes in v3:
time: 410 us; the launch traced here: 409 us
  waiting for transfers between devices  199 us (49%)
  starting transfers between devices  83.2 us (20%)
  matrix products  60.1 us (15%)
  other arithmetic  37.5 us (9%)
  local copies, waits for them, and re-layouts  22.5 us (5%)
  blocking collectives  6.37 us (2%)
    ppermute x25, waiting for transfers between devices, swap(): return lax.ppermute(value, axis, [(k, k ^ mask) for k in range(size)])  134 us
    ppermute x11, waiting for transfers between devices, gather_weight(): lax.ppermute(firsts[mask], 'grp', [(0, 1), (1, 0)])  65.1 us
    ppermute x25, starting transfers between devices, swap(): return lax.ppermute(value, axis, [(k, k ^ mask) for k in range(size)])  64.3 us
    dot_general x1, matrix products, layer(): pre_up = jnp.dot(normed_mid, full_up, preferred_element_type=jnp.float32)  31.9 us
    dot_general x4, matrix products, layer(): jnp.dot(hidden, jnp.concatenate([a, b]), preferred_element_type=jnp.float32)  17 us
    ppermute x11, starting transfers between devices, gather_weight(): lax.ppermute(firsts[mask], 'grp', [(0, 1), (1, 0)])  12.8 us
  transfers between devices with their start and end apart: 40, of which 15 were waited for; matrix products, arithmetic and copies ran while one was open for 26% of the time, Pallas kernels for 0%

profile of v3, /device:TPU:0, one launch (start us, length us, event | category | flops | bytes accessed | tf_op | source)
XLA Modules:
  0.0 409.4 jit_solution(383795935366922410)
XLA Ops:
  0.0 3.0 collective-permute-start.1
  6.0 1.6 collective-permute-start.3
  7.6 2.6 collective-permute-start.5
  12.0 1.8 slice_bitcast_fusion.14
  20.4 2.8 collective-permute-start.14
  25.1 2.5 collective-permute-start.17
  28.2 2.7 collective-permute-done.17
  30.9 2.5 collective-permute-start.7
  33.9 1.6 slice_bitcast_fusion.13
  35.6 1.5 collective-permute-start.4
  37.1 1.7 slice_bitcast_fusion.11
  42.1 2.8 collective-permute-done.4
  47.2 1.6 collective-permute-start.12
  49.6 2.2 collective-permute-start.15
  52.5 7.6 %collective-permute-done.12 = bf16[128,512]{1,0:T(8,128)(2,1)} collective-permute-done((bf16[128,512]{1,0:T(8,128)(2,1)S(1)}, bf16[128,512]{1,0:T(8,128)(2,1)}, u32[]{:S(2)}, u32[]{:S(2)}) %collective-permute-start.12) | collective-permute-done | bytes 131104 | tf_op jit(solution)/shard_map/ppermute | solution.py:12
  60.7 1.5 collective-permute-start.13
  65.5 1.6 pad_maximum_fusion
  68.2 2.4 fusion.152
  70.7 6.4 %all-reduce = (f32[1024]{0:T(1024)S(1)}, f32[1024]{0:T(1024)S(1)}) all-reduce(f32[1024]{0:T(1024)S(1)} %get-tuple-element.6, f32[1024]{0:T(1024)S(1)} %get-tuple-element.5), channel_id=1, replica_groups=mesh['grp'=2,'fs'=4,'tp'=4] {'tp'}, use_global_device_ids=true, to_apply=%region_7.8 | all-reduce | flops 2048 | bytes 16384 | tf_op jit(solution)/shard_map/psum | solution.py:160
  77.1 1.7 multiply_convert_fusion.9
  80.0 2.7 fusion.83
  88.3 1.7 dynamic-slice_bitcast_fusion.3
  91.0 2.5 convert_element_type.251
  95.0 2.7 collective-permute-start.26
  97.9 1.9 fusion.49
  100.7 2.5 convert_element_type.253
  104.6 1.7 collective-permute-start.28
  106.3 60.9 %collective-permute-done.26 = bf16[512,1024]{1,0:T(8,128)(2,1)} collective-permute-done((bf16[512,1024]{1,0:T(8,128)(2,1)}, bf16[512,1024]{1,0:T(8,128)(2,1)}, u32[]{:S(2)}, u32[]{:S(2)}) %collective-permute-start.26) | collective-permute-done | bytes 1048608 | tf_op jit(solution)/shard_map/ppermute | solution.py:12
  168.5 2.8 fusion.29
  171.9 1.6 collective-permute-start.34
  173.5 16.2 %collective-permute-done.32 = bf16[1024,512]{1,0:T(8,128)(2,1)} collective-permute-done((bf16[1024,512]{1,0:T(8,128)(2,1)}, bf16[1024,512]{1,0:T(8,128)(2,1)}, u32[]{:S(2)}, u32[]{:S(2)}) %collective-permute-start.32) | collective-permute-done | bytes 1048608 | tf_op jit(solution)/shard_map/ppermute | solution.py:12
  191.3 2.7 pad_maximum_fusion.5
  194.0 18.8 %collective-permute-start.24 = (bf16[512,1024]{1,0:T(8,128)(2,1)}, bf16[512,1024]{1,0:T(8,128)(2,1)}, u32[]{:S(2)}, u32[]{:S(2)}) collective-permute-start(bf16[512,1024]{1,0:T(8,128)(2,1)} %get-tuple-element.26), channel_id=1, source_target_pairs={{0,4},{4,0},{8,12},{12,8},{1,5},{5,1},{9,13},{13,9},{2,6},{6,2},{1... | collective-permute-start | bytes 3145736 | tf_op jit(solution)/shard_map/ppermute | solution.py:12
  214.9 20.0 %collective-permute-start.31 = (bf16[2048,512]{1,0:T(8,128)(2,1)S(1)}, bf16[2048,512]{1,0:T(8,128)(2,1)}, u32[]{:S(2)}, u32[]{:S(2)}) collective-permute-start(bf16[2048,512]{1,0:T(8,128)(2,1)S(1)} %copy-done.4), channel_id=1, source_target_pairs={{0,4},{4,0},{8,12},{12,8},{1,5},{5,1},{9,13},{13,9},{2,6},{6,2},{1... | collective-permute-start | bytes 6291464 | tf_op jit(solution)/shard_map/ppermute | solution.py:12
  236.3 2.4 broadcast_select_fusion
  238.9 17.8 %collective-permute-done.24 = bf16[512,1024]{1,0:T(8,128)(2,1)} collective-permute-done((bf16[512,1024]{1,0:T(8,128)(2,1)}, bf16[512,1024]{1,0:T(8,128)(2,1)}, u32[]{:S(2)}, u32[]{:S(2)}) %collective-permute-start.24) | collective-permute-done | bytes 1048608 | tf_op jit(solution)/shard_map/ppermute | solution.py:12
  260.3 1.6 collective-permute-start.30
  262.1 1.6 pad_maximum_fusion.3
  263.7 2.3 fusion.48
  266.6 38.9 %collective-permute-done.25 = bf16[512,1024]{1,0:T(8,128)(2,1)S(1)} collective-permute-done((bf16[512,1024]{1,0:T(8,128)(2,1)}, bf16[512,1024]{1,0:T(8,128)(2,1)S(1)}, u32[]{:S(2)}, u32[]{:S(2)}) %collective-permute-start.25) | collective-permute-done | bytes 1048608 | tf_op jit(solution)/shard_map/ppermute | solution.py:40
  305.5 22.5 %collective-permute-done.30 = bf16[512,1024]{1,0:T(8,128)(2,1)S(1)} collective-permute-done((bf16[512,1024]{1,0:T(8,128)(2,1)S(1)}, bf16[512,1024]{1,0:T(8,128)(2,1)S(1)}, u32[]{:S(2)}, u32[]{:S(2)}) %collective-permute-start.30) | collective-permute-done | bytes 1048608 | tf_op jit(solution)/shard_map/ppermute | solution.py:40
  328.9 31.9 %multiply_convert_fusion = bf16[1024,2048]{1,0:T(8,128)(2,1)} fusion(f32[2048]{0:T(1024)S(1)} %pad_maximum_fusion.8, bf16[512,1024]{1,0:T(8,128)(2,1)} %copy-done.36, bf16[512,1024]{1,0:T(8,128)(2,1)} %copy-done.10, bf16[512,1024]{1,0:T(8,128)(2,1)} %copy-done.34, bf16[512,1024]{1,0:T(8,128)(2,1)} %collective-permute-done.26, ...), kind=kOutput, calls=%fused_computation.16 | convolution fusion | flops 8682209280 | bytes 16785408 | tf_op jit(solution)/shard_map/dot_general | solution.py:192
  360.9 5.0 %fusion.67 = bf16[1,1024,512]{1,2,0:T(8,128)(2,1)S(1)} fusion(bf16[1024,2048]{1,0:T(8,128)(2,1)} %multiply_convert_fusion, f32[512]{0:T(512)S(1)} %copy-done.27, bf16[1024,512]{1,0:T(8,128)(2,1)S(1)} %get-tuple-element.23, bf16[1024,512]{1,0:T(8,128)(2,1)} %get-tuple-element.24), kind=kOutput, calls=%fused_computation.98 | convolution fusion | flops 2152726528 | bytes 7342080 | tf_op jit(solution)/shard_map/dot_general | solution.py:196
  366.0 4.0 fusion.69
  370.0 4.0 fusion.68
  374.0 4.0 fusion.72
  379.4 2.1 collective-permute-done.38
  383.0 24.2 %collective-permute-done.39 = bf16[1024,512]{0,1:T(8,128)(2,1)S(1)} collective-permute-done((bf16[1024,512]{0,1:T(8,128)(2,1)S(1)}, bf16[1024,512]{0,1:T(8,128)(2,1)S(1)}, u32[]{:S(2)}, u32[]{:S(2)}) %collective-permute-start.39) | collective-permute-done | bytes 1048608 | tf_op jit(solution)/shard_map/ppermute | solution.py:12
  (179 shorter events, 55.6 us)
Async XLA Ops:
  0.0 46.5 %collective-permute-start.1 = (bf16[1024,512]{1,0:T(8,128)(2,1)}, bf16[1024,512]{1,0:T(8,128)(2,1)S(1)}, u32[]{:S(2)}, u32[]{:S(2)}) collective-permute-start(bf16[1024,512]{1,0:T(8,128)(2,1)} %param.16), channel_id=1, source_target_pairs={{0,2},{1,3},{2,0},{3,1},{4,6},{5,7},{6,4},{7,5},{8,10},{9,11},{10,... | collective-permute-start | bytes 3145736 | tf_op jit(solution)/shard_map/ppermute | solution.py:12
  3.1 60.6 %collective-permute-start = (bf16[1024,512]{1,0:T(8,128)(2,1)}, bf16[1024,512]{1,0:T(8,128)(2,1)}, u32[]{:S(2)}, u32[]{:S(2)}) collective-permute-start(bf16[1024,512]{1,0:T(8,128)(2,1)} %param.16), channel_id=1, source_target_pairs={{0,1},{1,0},{2,3},{3,2},{4,5},{5,4},{6,7},{7,6},{8,9},{9,8},{10,11... | collective-permute-start | bytes 3145736 | tf_op jit(solution)/shard_map/ppermute | solution.py:12
  6.0 27.9 %collective-permute-start.3 = (bf16[512,2,128]{2,0,1:T(8,128)(2,1)S(1)}, bf16[512,2,128]{2,0,1:T(8,128)(2,1)}, u32[]{:S(2)}, u32[]{:S(2)}) collective-permute-start(bf16[512,2,128]{2,0,1:T(8,128)(2,1)S(1)} %get-tuple-element.28), channel_id=1, source_target_pairs={{0,4},{4,0},{8,12},{12,8},{1,5},{5,1},{9,13},{13,9},{2,6},{6,2},{1... | collective-permute-start | bytes 786440 | tf_op jit(solution)/shard_map/ppermute | solution.py:12
  7.6 28.0 %collective-permute-start.5 = (bf16[512,2,128]{2,0,1:T(8,128)(2,1)S(1)}, bf16[512,2,128]{2,0,1:T(8,128)(2,1)}, u32[]{:S(2)}, u32[]{:S(2)}) collective-permute-start(bf16[512,2,128]{2,0,1:T(8,128)(2,1)S(1)} %get-tuple-element.28), channel_id=1, source_target_pairs={{0,8},{4,12},{8,0},{12,4},{1,9},{5,13},{9,1},{13,5},{2,10},{6,14},... | collective-permute-start | bytes 786440 | tf_op jit(solution)/shard_map/ppermute | solution.py:12
  10.8 9.6 %collective-permute-start.11 = (f32[2,512]{1,0:T(2,128)}, f32[2,512]{1,0:T(2,128)}, u32[]{:S(2)}, u32[]{:S(2)}) collective-permute-start(f32[2,512]{1,0:T(2,128)} %pad_maximum_fusion.9), channel_id=1, source_target_pairs={{0,4},{4,0},{8,12},{12,8},{1,5},{5,1},{9,13},{13,9},{2,6},{6,2},{1... | collective-permute-start | bytes 12296 | tf_op jit(solution)/shard_map/ppermute | solution.py:12
  20.2 27.0 %copy-start.11 = (bf16[128,512]{1,0:T(8,128)(2,1)S(1)}, bf16[128,512]{1,0:T(8,128)(2,1)}, u32[]{:S(2)}) copy-start(bf16[128,512]{1,0:T(8,128)(2,1)} %get-tuple-element.30) | copy-start | bytes 393220
  20.4 4.7 %collective-permute-start.14 = (f32[2,512]{1,0:T(2,128)}, f32[2,512]{1,0:T(2,128)S(1)}, u32[]{:S(2)}, u32[]{:S(2)}) collective-permute-start(f32[2,512]{1,0:T(2,128)} %pad_maximum_fusion.9), channel_id=1, source_target_pairs={{0,8},{4,12},{8,0},{12,4},{1,9},{5,13},{9,1},{13,5},{2,10},{6,14},... | collective-permute-start | bytes 12296 | tf_op jit(solution)/shard_map/ppermute | solution.py:12
  25.1 5.7 %collective-permute-start.17 = (f32[2,512]{1,0:T(2,128)}, f32[2,512]{1,0:T(2,128)S(1)}, u32[]{:S(2)}, u32[]{:S(2)}) collective-permute-start(f32[2,512]{1,0:T(2,128)} %pad_maximum_fusion.9), channel_id=1, source_target_pairs={{0,12},{4,8},{8,4},{12,0},{1,13},{5,9},{9,5},{13,1},{2,14},{6,10},... | collective-permute-start | bytes 12296 | tf_op jit(solution)/shard_map/ppermute | solution.py:12
  30.9 9.1 %collective-permute-start.7 = (bf16[512,2,128]{2,0,1:T(8,128)(2,1)S(1)}, bf16[512,2,128]{2,0,1:T(8,128)(2,1)S(1)}, u32[]{:S(2)}, u32[]{:S(2)}) collective-permute-start(bf16[512,2,128]{2,0,1:T(8,128)(2,1)S(1)} %get-tuple-element.28), channel_id=1, source_target_pairs={{0,12},{4,8},{8,4},{12,0},{1,13},{5,9},{9,5},{13,1},{2,14},{6,10},... | collective-permute-start | bytes 786440 | tf_op jit(solution)/shard_map/ppermute | solution.py:12
  33.9 13.2 %collective-permute-start.9 = (bf16[128,512]{1,0:T(8,128)(2,1)}, bf16[128,512]{1,0:T(8,128)(2,1)}, u32[]{:S(2)}, u32[]{:S(2)}) collective-permute-start(bf16[128,512]{1,0:T(8,128)(2,1)} %get-tuple-element.30), channel_id=1, source_target_pairs={{0,4},{4,0},{8,12},{12,8},{1,5},{5,1},{9,13},{13,9},{2,6},{6,2},{1... | collective-permute-start | bytes 393224 | tf_op jit(solution)/shard_map/ppermute | solution.py:12
  35.6 9.4 %collective-permute-start.4 = (bf16[512,2,128]{2,0,1:T(8,128)(2,1)}, bf16[512,2,128]{2,0,1:T(8,128)(2,1)S(1)}, u32[]{:S(2)}, u32[]{:S(2)}) collective-permute-start(bf16[512,2,128]{2,0,1:T(8,128)(2,1)} %collective-permute-done.3), channel_id=1, source_target_pairs={{0,16},{16,0},{1,17},{17,1},{2,18},{18,2},{3,19},{19,3},{4,20},{20... | collective-permute-start | bytes 786440 | tf_op jit(solution)/shard_map/ppermute | solution.py:40
  39.9 9.7 %collective-permute-start.6 = (bf16[512,2,128]{2,0,1:T(8,128)(2,1)}, bf16[512,2,128]{2,0,1:T(8,128)(2,1)S(1)}, u32[]{:S(2)}, u32[]{:S(2)}) collective-permute-start(bf16[512,2,128]{2,0,1:T(8,128)(2,1)} %collective-permute-done.5), channel_id=1, source_target_pairs={{0,16},{16,0},{1,17},{17,1},{2,18},{18,2},{3,19},{19,3},{4,20},{20... | collective-permute-start | bytes 786440 | tf_op jit(solution)/shard_map/ppermute | solution.py:40
  45.0 17.2 %collective-permute-start.8 = (bf16[512,2,128]{2,0,1:T(8,128)(2,1)S(1)}, bf16[512,2,128]{2,0,1:T(8,128)(2,1)S(1)}, u32[]{:S(2)}, u32[]{:S(2)}) collective-permute-start(bf16[512,2,128]{2,0,1:T(8,128)(2,1)S(1)} %collective-permute-done.7), channel_id=1, source_target_pairs={{0,16},{16,0},{1,17},{17,1},{2,18},{18,2},{3,19},{19,3},{4,20},{20... | collective-permute-start | bytes 786440 | tf_op jit(solution)/shard_map/ppermute | solution.py:40
  46.5 18.7 %collective-permute-start.2 = (bf16[1024,512]{1,0:T(8,128)(2,1)S(1)}, bf16[1024,512]{1,0:T(8,128)(2,1)S(1)}, u32[]{:S(2)}, u32[]{:S(2)}) collective-permute-start(bf16[1024,512]{1,0:T(8,128)(2,1)S(1)} %collective-permute-done.1), channel_id=1, source_target_pairs={{0,1},{1,0},{2,3},{3,2},{4,5},{5,4},{6,7},{7,6},{8,9},{9,8},{10,11... | collective-permute-start | bytes 3145736 | tf_op jit(solution)/shard_map/ppermute | solution.py:12
  47.2 13.0 %collective-permute-start.12 = (bf16[128,512]{1,0:T(8,128)(2,1)S(1)}, bf16[128,512]{1,0:T(8,128)(2,1)}, u32[]{:S(2)}, u32[]{:S(2)}) collective-permute-start(bf16[128,512]{1,0:T(8,128)(2,1)S(1)} %copy-done.11), channel_id=1, source_target_pairs={{0,8},{4,12},{8,0},{12,4},{1,9},{5,13},{9,1},{13,5},{2,10},{6,14},... | collective-permute-start | bytes 393224 | tf_op jit(solution)/shard_map/ppermute | solution.py:12
  49.6 11.0 %collective-permute-start.15 = (bf16[128,512]{1,0:T(8,128)(2,1)S(1)}, bf16[128,512]{1,0:T(8,128)(2,1)}, u32[]{:S(2)}, u32[]{:S(2)}) collective-permute-start(bf16[128,512]{1,0:T(8,128)(2,1)S(1)} %copy-done.11), channel_id=1, source_target_pairs={{0,12},{4,8},{8,4},{12,0},{1,13},{5,9},{9,5},{13,1},{2,14},{6,10},... | collective-permute-start | bytes 393224 | tf_op jit(solution)/shard_map/ppermute | solution.py:12
  60.2 23.1 %collective-permute-start.10 = (bf16[128,512]{1,0:T(8,128)(2,1)}, bf16[128,512]{1,0:T(8,128)(2,1)}, u32[]{:S(2)}, u32[]{:S(2)}) collective-permute-start(bf16[128,512]{1,0:T(8,128)(2,1)} %collective-permute-done.9), channel_id=1, source_target_pairs={{0,16},{16,0},{1,17},{17,1},{2,18},{18,2},{3,19},{19,3},{4,20},{20... | collective-permute-start | bytes 393224 | tf_op jit(solution)/shard_map/ppermute | solution.py:40
  60.7 24.1 %collective-permute-start.13 = (bf16[128,512]{1,0:T(8,128)(2,1)}, bf16[128,512]{1,0:T(8,128)(2,1)}, u32[]{:S(2)}, u32[]{:S(2)}) collective-permute-start(bf16[128,512]{1,0:T(8,128)(2,1)} %collective-permute-done.12), channel_id=1, source_target_pairs={{0,16},{16,0},{1,17},{17,1},{2,18},{18,2},{3,19},{19,3},{4,20},{20... | collective-permute-start | bytes 393224 | tf_op jit(solution)/shard_map/ppermute | solution.py:40
  62.2 24.1 %collective-permute-start.16 = (bf16[128,512]{1,0:T(8,128)(2,1)}, bf16[128,512]{1,0:T(8,128)(2,1)}, u32[]{:S(2)}, u32[]{:S(2)}) collective-permute-start(bf16[128,512]{1,0:T(8,128)(2,1)} %collective-permute-done.15), channel_id=1, source_target_pairs={{0,16},{16,0},{1,17},{17,1},{2,18},{18,2},{3,19},{19,3},{4,20},{20... | collective-permute-start | bytes 393224 | tf_op jit(solution)/shard_map/ppermute | solution.py:40
  91.0 6.9 %collective-permute-start.19 = (bf16[1024,512]{0,1:T(8,128)(2,1)}, bf16[1024,512]{0,1:T(8,128)(2,1)}, u32[]{:S(2)}, u32[]{:S(2)}) collective-permute-start(bf16[1024,512]{0,1:T(8,128)(2,1)} %get-tuple-element.22), channel_id=1, source_target_pairs={{0,1},{1,0},{2,3},{3,2},{4,5},{5,4},{6,7},{7,6},{8,9},{9,8},{10,11... | collective-permute-start | bytes 3145736 | tf_op jit(solution)/shard_map/ppermute | solution.py:12
  95.0 72.2 %collective-permute-start.26 = (bf16[512,1024]{1,0:T(8,128)(2,1)}, bf16[512,1024]{1,0:T(8,128)(2,1)}, u32[]{:S(2)}, u32[]{:S(2)}) collective-permute-start(bf16[512,1024]{1,0:T(8,128)(2,1)} %get-tuple-element.26), channel_id=1, source_target_pairs={{0,8},{4,12},{8,0},{12,4},{1,9},{5,13},{9,1},{13,5},{2,10},{6,14},... | collective-permute-start | bytes 3145736 | tf_op jit(solution)/shard_map/ppermute | solution.py:12
  97.7 70.8 %collective-permute-start.18 = (bf16[1024,512]{0,1:T(8,128)(2,1)}, bf16[1024,512]{0,1:T(8,128)(2,1)}, u32[]{:S(2)}, u32[]{:S(2)}) collective-permute-start(bf16[1024,512]{0,1:T(8,128)(2,1)} %get-tuple-element.21), channel_id=1, source_target_pairs={{0,1},{1,0},{2,3},{3,2},{4,5},{5,4},{6,7},{7,6},{8,9},{9,8},{10,11... | collective-permute-start | bytes 3145736 | tf_op jit(solution)/shard_map/ppermute | solution.py:12
  99.9 68.6 %collective-permute-start.20 = (bf16[1024,512]{0,1:T(8,128)(2,1)S(1)}, bf16[1024,512]{0,1:T(8,128)(2,1)}, u32[]{:S(2)}, u32[]{:S(2)}) collective-permute-start(bf16[1024,512]{0,1:T(8,128)(2,1)S(1)} %fusion.49), channel_id=1, source_target_pairs={{0,2},{1,3},{2,0},{3,1},{4,6},{5,7},{6,4},{7,5},{8,10},{9,11},{10,... | collective-permute-start | bytes 3145736 | tf_op jit(solution)/shard_map/ppermute | solution.py:12
  104.3 85.4 %collective-permute-start.32 = (bf16[1024,512]{1,0:T(8,128)(2,1)}, bf16[1024,512]{1,0:T(8,128)(2,1)}, u32[]{:S(2)}, u32[]{:S(2)}) collective-permute-start(bf16[1024,512]{1,0:T(8,128)(2,1)} %get-tuple-element.24), channel_id=1, source_target_pairs={{0,8},{4,12},{8,0},{12,4},{1,9},{5,13},{9,1},{13,5},{2,10},{6,14},... | collective-permute-start | bytes 3145736 | tf_op jit(solution)/shard_map/ppermute | solution.py:12
  104.6 89.3 %collective-permute-start.28 = (bf16[512,1024]{1,0:T(8,128)(2,1)}, bf16[512,1024]{1,0:T(8,128)(2,1)}, u32[]{:S(2)}, u32[]{:S(2)}) collective-permute-start(bf16[512,1024]{1,0:T(8,128)(2,1)} %get-tuple-element.26), channel_id=1, source_target_pairs={{4,8},{8,4},{5,9},{9,5},{6,10},{10,6},{7,11},{11,7},{20,24},{24,20... | collective-permute-start | bytes 3145736 | tf_op jit(solution)/shard_map/ppermute | solution.py:20
  167.2 45.6 %collective-permute-start.29 = (bf16[512,1024]{1,0:T(8,128)(2,1)}, bf16[512,1024]{1,0:T(8,128)(2,1)}, u32[]{:S(2)}, u32[]{:S(2)}) collective-permute-start(bf16[512,1024]{1,0:T(8,128)(2,1)} %collective-permute-done.26), channel_id=1, source_target_pairs={{4,0},{8,12},{5,1},{9,13},{6,2},{10,14},{7,3},{11,15},{20,16},{24,... | collective-permute-start | bytes 3145736 | tf_op jit(solution)/shard_map/ppermute | solution.py:21
  171.3 41.5 %collective-permute-start.22 = (bf16[1024,512]{0,1:T(8,128)(2,1)S(1)}, bf16[1024,512]{0,1:T(8,128)(2,1)S(1)}, u32[]{:S(2)}, u32[]{:S(2)}) collective-permute-start(bf16[1024,512]{0,1:T(8,128)(2,1)S(1)} %get-tuple-element.10), channel_id=1, source_target_pairs={{0,2},{1,3},{2,0},{3,1},{4,6},{5,7},{6,4},{7,5},{8,10},{9,11},{10,... | collective-permute-start | bytes 3145736 | tf_op jit(solution)/shard_map/ppermute | solution.py:12
  171.9 43.0 %collective-permute-start.34 = (bf16[1024,512]{1,0:T(8,128)(2,1)}, bf16[1024,512]{1,0:T(8,128)(2,1)}, u32[]{:S(2)}, u32[]{:S(2)}) collective-permute-start(bf16[1024,512]{1,0:T(8,128)(2,1)} %get-tuple-element.24), channel_id=1, source_target_pairs={{4,8},{8,4},{5,9},{9,5},{6,10},{10,6},{7,11},{11,7},{20,24},{24,20... | collective-permute-start | bytes 3145736 | tf_op jit(solution)/shard_map/ppermute | solution.py:20
  189.7 45.1 %collective-permute-start.35 = (bf16[1024,512]{1,0:T(8,128)(2,1)}, bf16[1024,512]{1,0:T(8,128)(2,1)}, u32[]{:S(2)}, u32[]{:S(2)}) collective-permute-start(bf16[1024,512]{1,0:T(8,128)(2,1)} %collective-permute-done.32), channel_id=1, source_target_pairs={{4,0},{8,12},{5,1},{9,13},{6,2},{10,14},{7,3},{11,15},{20,16},{24,... | collective-permute-start | bytes 3145736 | tf_op jit(solution)/shard_map/ppermute | solution.py:21
  191.2 21.5 %copy-start.18 = (f32[2048]{0:T(1024)S(1)}, f32[2048]{0:T(1024)}, u32[]{:S(2)}) copy-start(f32[2048]{0:T(1024)} %param.27) | copy-start | bytes 24580
  191.2 21.6 %copy-start.19 = (f32[2048]{0:T(1024)S(1)}, f32[2048]{0:T(1024)}, u32[]{:S(2)}) copy-start(f32[2048]{0:T(1024)} %param.29) | copy-start | bytes 24580
  194.0 62.8 %collective-permute-start.24 = (bf16[512,1024]{1,0:T(8,128)(2,1)}, bf16[512,1024]{1,0:T(8,128)(2,1)}, u32[]{:S(2)}, u32[]{:S(2)}) collective-permute-start(bf16[512,1024]{1,0:T(8,128)(2,1)} %get-tuple-element.26), channel_id=1, source_target_pairs={{0,4},{4,0},{8,12},{12,8},{1,5},{5,1},{9,13},{13,9},{2,6},{6,2},{1... | collective-permute-start | bytes 3145736 | tf_op jit(solution)/shard_map/ppermute | solution.py:12
  212.8 45.5 %collective-permute-start.21 = (bf16[1024,512]{0,1:T(8,128)(2,1)S(1)}, bf16[1024,512]{0,1:T(8,128)(2,1)}, u32[]{:S(2)}, u32[]{:S(2)}) collective-permute-start(bf16[1024,512]{0,1:T(8,128)(2,1)S(1)} %get-tuple-element.10), channel_id=1, source_target_pairs={{0,1},{1,0},{2,3},{3,2},{4,5},{5,4},{6,7},{7,6},{8,9},{9,8},{10,11... | collective-permute-start | bytes 3145736 | tf_op jit(solution)/shard_map/ppermute | solution.py:12
  212.9 47.4 %collective-permute-start.23 = (bf16[1024,512]{0,1:T(8,128)(2,1)S(1)}, bf16[1024,512]{0,1:T(8,128)(2,1)S(1)}, u32[]{:S(2)}, u32[]{:S(2)}) collective-permute-start(bf16[1024,512]{0,1:T(8,128)(2,1)S(1)} %collective-permute-done.22), channel_id=1, source_target_pairs={{0,1},{1,0},{2,3},{3,2},{4,5},{5,4},{6,7},{7,6},{8,9},{9,8},{10,11... | collective-permute-start | bytes 3145736 | tf_op jit(solution)/shard_map/ppermute | solution.py:12
  214.8 45.4 %copy-start.10 = (bf16[512,1024]{1,0:T(8,128)(2,1)}, bf16[512,1024]{1,0:T(8,128)(2,1)S(1)}, u32[]{:S(2)}) copy-start(bf16[512,1024]{1,0:T(8,128)(2,1)S(1)} %broadcast_select_fusion.1) | copy-start | bytes 3145732
  214.9 155.1 %collective-permute-start.31 = (bf16[2048,512]{1,0:T(8,128)(2,1)S(1)}, bf16[2048,512]{1,0:T(8,128)(2,1)}, u32[]{:S(2)}, u32[]{:S(2)}) collective-permute-start(bf16[2048,512]{1,0:T(8,128)(2,1)S(1)} %copy-done.4), channel_id=1, source_target_pairs={{0,4},{4,0},{8,12},{12,8},{1,5},{5,1},{9,13},{13,9},{2,6},{6,2},{1... | collective-permute-start | bytes 6291464 | tf_op jit(solution)/shard_map/ppermute | solution.py:12
  234.8 31.2 %collective-permute-start.27 = (bf16[512,1024]{1,0:T(8,128)(2,1)}, bf16[512,1024]{1,0:T(8,128)(2,1)S(1)}, u32[]{:S(2)}, u32[]{:S(2)}) collective-permute-start(bf16[512,1024]{1,0:T(8,128)(2,1)} %collective-permute-done.26), channel_id=1, source_target_pairs={{0,16},{16,0},{1,17},{17,1},{2,18},{18,2},{3,19},{19,3},{4,20},{20... | collective-permute-start | bytes 3145736 | tf_op jit(solution)/shard_map/ppermute | solution.py:40
  256.8 109.2 %collective-permute-start.33 = (bf16[1024,512]{1,0:T(8,128)(2,1)}, bf16[1024,512]{1,0:T(8,128)(2,1)}, u32[]{:S(2)}, u32[]{:S(2)}) collective-permute-start(bf16[1024,512]{1,0:T(8,128)(2,1)} %collective-permute-done.32), channel_id=1, source_target_pairs={{0,16},{16,0},{1,17},{17,1},{2,18},{18,2},{3,19},{19,3},{4,20},{20... | collective-permute-start | bytes 3145736 | tf_op jit(solution)/shard_map/ppermute | solution.py:40
  258.3 47.2 %collective-permute-start.25 = (bf16[512,1024]{1,0:T(8,128)(2,1)}, bf16[512,1024]{1,0:T(8,128)(2,1)S(1)}, u32[]{:S(2)}, u32[]{:S(2)}) collective-permute-start(bf16[512,1024]{1,0:T(8,128)(2,1)} %collective-permute-done.24), channel_id=1, source_target_pairs={{0,16},{16,0},{1,17},{17,1},{2,18},{18,2},{3,19},{19,3},{4,20},{20... | collective-permute-start | bytes 3145736 | tf_op jit(solution)/shard_map/ppermute | solution.py:40
  260.3 67.7 %collective-permute-start.30 = (bf16[512,1024]{1,0:T(8,128)(2,1)S(1)}, bf16[512,1024]{1,0:T(8,128)(2,1)S(1)}, u32[]{:S(2)}, u32[]{:S(2)}) collective-permute-start(bf16[512,1024]{1,0:T(8,128)(2,1)S(1)} %broadcast_select_fusion.1), channel_id=1, source_target_pairs={{0,16},{16,0},{1,17},{17,1},{2,18},{18,2},{3,19},{19,3},{4,20},{20... | collective-permute-start | bytes 3145736 | tf_op jit(solution)/shard_map/ppermute | solution.py:40
  263.7 65.2 %copy-start.5 = (bf16[512,1024]{1,0:T(8,128)(2,1)S(1)}, bf16[512,1024]{1,0:T(8,128)(2,1)}, u32[]{:S(2)}) copy-start(bf16[512,1024]{1,0:T(8,128)(2,1)} %get-tuple-element.25) | copy-start | bytes 3145732
  266.0 62.0 %copy-start.34 = (bf16[512,1024]{1,0:T(8,128)(2,1)}, bf16[512,1024]{1,0:T(8,128)(2,1)S(1)}, u32[]{:S(2)}) copy-start(bf16[512,1024]{1,0:T(8,128)(2,1)S(1)} %collective-permute-done.27) | copy-start | bytes 3145732
  266.0 108.0 %collective-permute-start.36 = (bf16[1024,512]{1,0:T(8,128)(2,1)}, bf16[1024,512]{1,0:T(8,128)(2,1)}, u32[]{:S(2)}, u32[]{:S(2)}) collective-permute-start(bf16[1024,512]{1,0:T(8,128)(2,1)} %broadcast_select_fusion), channel_id=1, source_target_pairs={{0,16},{16,0},{1,17},{17,1},{2,18},{18,2},{3,19},{19,3},{4,20},{20... | collective-permute-start | bytes 3145736 | tf_op jit(solution)/shard_map/ppermute | solution.py:40
  305.5 22.5 %copy-start.35 = (bf16[512,1024]{1,0:T(8,128)(2,1)}, bf16[512,1024]{1,0:T(8,128)(2,1)S(1)}, u32[]{:S(2)}) copy-start(bf16[512,1024]{1,0:T(8,128)(2,1)S(1)} %collective-permute-done.25) | copy-start | bytes 3145732
  328.9 32.0 %copy-start.27 = (f32[512]{0:T(512)S(1)}, f32[512]{0:T(512)}, u32[]{:S(2)}) copy-start(f32[512]{0:T(512)} %param.31) | copy-start | bytes 6148
  378.8 2.7 collective-permute-start.38
  378.9 4.1 %collective-permute-start.37 = (bf16[1024,512]{0,1:T(8,128)(2,1)S(1)}, bf16[1024,512]{0,1:T(8,128)(2,1)S(1)}, u32[]{:S(2)}, u32[]{:S(2)}) collective-permute-start(bf16[1024,512]{0,1:T(8,128)(2,1)S(1)} %get-tuple-element.19), channel_id=1, source_target_pairs={{0,1},{1,0},{2,3},{3,2},{4,5},{5,4},{6,7},{7,6},{8,9},{9,8},{10,11... | collective-permute-start | bytes 3145736 | tf_op jit(solution)/shard_map/ppermute | solution.py:12
  381.9 25.3 %collective-permute-start.39 = (bf16[1024,512]{0,1:T(8,128)(2,1)S(1)}, bf16[1024,512]{0,1:T(8,128)(2,1)S(1)}, u32[]{:S(2)}, u32[]{:S(2)}) collective-permute-start(bf16[1024,512]{0,1:T(8,128)(2,1)S(1)} %fusion.39), channel_id=1, source_target_pairs={{0,2},{1,3},{2,0},{3,1},{4,6},{5,7},{6,4},{7,5},{8,10},{9,11},{10,... | collective-permute-start | bytes 3145736 | tf_op jit(solution)/shard_map/ppermute | solution.py:12
  (30 other events, 136.5 us)
